TPU v7x, 32 devices: a whole 2x2x4 slice. The times are simulated.
32 devices in a mesh: sp: 8 (over z, y), tp: 4 (over x, core).
Axes of the slice: x: 2, y: 2, z: 4, core: 2. Of those that a mesh axis runs over, the one named last changes fastest.
Arguments:
- queries: bfloat16 [4096, 512], P('sp', 'tp'), may hold values from -6 to 6
- key_matrix: bfloat16 [4096, 512], P('sp', 'tp'), may hold values from -6 to 6
- value_matrix: bfloat16 [4096, 1024], P('sp', 'tp'), may hold values from -6 to 6
- channel_decay_input: bfloat16 [4096, 512], P('sp', 'tp')
- head_decay_offset: float32 [4096, 8], P('sp', 'tp'), may hold values from -1 to 0
- output_gate_input: bfloat16 [4096, 1024], P('sp', 'tp'), may hold values from -6 to 6
- head_norm_gain: float32 [128], replicated, may hold values from 0.1 to 1.9
- residual: bfloat16 [4096, 2048], P(('sp', 'tp')), may hold values from -6 to 6
- mixer_output_weight: bfloat16 [1024, 2048], replicated, may hold values from -0.1875 to 0.1875
- expert_norm_gain: float32 [2048], replicated, may hold values from 0.1 to 1.9
- routes: int32 [4096, 4], P(('sp', 'tp')), may hold values from 0 to 63, all different within a row; in each aligned block of 128 rows (0 to 127, 128 to 255, ...) at most 16 rows name the same one
- chosen_router_scores: float32 [4096, 4], P(('sp', 'tp')), may hold values from 0.1 to 1
- routed_gate_weight: bfloat16 [64, 2048, 512], P(('sp', 'tp')), may hold values from -0.125 to 0.125
- routed_up_weight: bfloat16 [64, 2048, 512], P(('sp', 'tp')), may hold values from -0.125 to 0.125
- routed_down_weight: bfloat16 [64, 512, 2048], P(('sp', 'tp')), may hold values from -0.25 to 0.25
- common_gate_weight: bfloat16 [2048, 512], replicated, may hold values from -0.125 to 0.125
- common_up_weight: bfloat16 [2048, 512], replicated, may hold values from -0.125 to 0.125
- common_down_weight: bfloat16 [512, 2048], replicated, may hold values from -0.25 to 0.25
Outputs:
- layer_out: bfloat16 [4096, 2048], P(('sp', 'tp'))
Inputs may be any that keep to these rules, and one draw needn't show every extreme that they name: `routes`: each row names 4 different experts. In each aligned block of 128 rows (the rows of one device) no expert is named by more than 16 rows, a bound that some block reaches.
All inputs are finite; a program needn't handle non-finite values.
Results may differ from a plain program's by a relative error of at most 0.017.
Values may be sent and summed in bfloat16 or wider, within the bound.
A program may use at most 128 MiB of HBM per device.

v0:
```python
import functools
import math

import jax
import jax.numpy as jnp
from jax import lax
from jax.experimental import pallas as pl
from jax.experimental.pallas import tpu as pltpu
from jax.sharding import PartitionSpec as P

D = 2048
KEY_CHANNELS = 64
VDIM = 128
BLOCK = 64
TOP_K = 4


eps_norm = 1e-06
decay_running = 16.0
routed_scale = 2.5


def peer(sp, tp):
    return {"sp": sp, "tp": tp}


def greet(targets):
    barrier = pltpu.get_barrier_semaphore()
    for target in targets:
        pl.semaphore_signal(
            barrier, inc=1, device_id=target, device_id_type=pl.DeviceIdType.MESH
        )
    pl.semaphore_wait(barrier, len(targets))


def remote(src, dst, send, recv, target):
    return pltpu.make_async_remote_copy(
        src_ref=src,
        dst_ref=dst,
        send_sem=send,
        recv_sem=recv,
        device_id=target,
        device_id_type=pl.DeviceIdType.MESH,
    )


def remote_call(kernel, out_shape, operands, scratch, number, flops=1_000_000):
    multi = isinstance(out_shape, (tuple, list))
    vmem = pl.BlockSpec(memory_space=pltpu.VMEM)
    return pl.pallas_call(
        kernel,
        out_shape=out_shape,
        in_specs=[vmem] * len(operands),
        out_specs=[vmem] * len(out_shape) if multi else vmem,
        scratch_shapes=scratch,
        compiler_params=pltpu.CompilerParams(
            collective_id=number, has_side_effects=True, vmem_limit_bytes=56 * 1024 * 1024
        ),
    )(*operands)


def gather_sp_kernel(count, x_ref, y_ref, xs_ref, ys_ref, send, recv):
    me, tp = lax.axis_index("sp"), lax.axis_index("tp")
    targets = [peer(lax.rem(me + d, count), tp) for d in range(1, count)]
    greet(targets)
    copies = []
    for d in range(1, count):
        for i, (src, dst) in enumerate(((x_ref, xs_ref), (y_ref, ys_ref))):
            copies.append(
                remote(src, dst.at[me], send.at[i, d], recv.at[i, d], targets[d - 1])
            )
            copies[-1].start()
    xs_ref[me] = x_ref[...]
    ys_ref[me] = y_ref[...]
    for copy in copies:
        copy.wait()


def gather_sp(state, packet):
    count = lax.axis_size("sp")
    return remote_call(
        functools.partial(gather_sp_kernel, count),
        [
            jax.ShapeDtypeStruct((count,) + state.shape, state.dtype),
            jax.ShapeDtypeStruct((count,) + packet.shape, packet.dtype),
        ],
        [state, packet],
        [pltpu.SemaphoreType.DMA((2, count)), pltpu.SemaphoreType.DMA((2, count))],
        0,
    )


def swap_tp_kernel(count, x_ref, out_ref, send, recv):
    sp, me = lax.axis_index("sp"), lax.axis_index("tp")
    width = x_ref.shape[2]
    targets = [peer(sp, lax.rem(me + d, count)) for d in range(1, count)]
    greet(targets)
    columns = pl.ds(pl.multiple_of(me * width, width), width)
    copies = []
    for d in range(1, count):
        copies.append(
            remote(
                x_ref.at[lax.rem(me + d, count)],
                out_ref.at[:, columns],
                send.at[d],
                recv.at[d],
                targets[d - 1],
            )
        )
        copies[-1].start()
    out_ref[:, columns] = x_ref[me]
    for copy in copies:
        copy.wait()


def swap_tp(stacked):
    count = lax.axis_size("tp")
    return remote_call(
        functools.partial(swap_tp_kernel, count),
        jax.ShapeDtypeStruct((stacked.shape[1], count * stacked.shape[2]), stacked.dtype),
        [stacked],
        [pltpu.SemaphoreType.DMA((count,)), pltpu.SemaphoreType.DMA((count,))],
        1,
    )


class Place:
    def __init__(self, sp_size, tp_size):
        self.deep = math.gcd(sp_size, 4)
        self.rows = sp_size // self.deep
        self.tp_size = tp_size
        self.flat = self.rows * tp_size

    def here(self):
        sp, tp = lax.axis_index("sp"), lax.axis_index("tp")
        self.sp, self.tp = sp, tp
        self.a = sp // self.rows
        self.b = lax.rem(sp, self.rows)
        self.p = self.b * self.tp_size + tp
        return self

    def column(self, a):
        return peer(a * self.rows + self.b, self.tp)

    def plane(self, p):
        return peer(self.a * self.rows + p // self.tp_size, lax.rem(p, self.tp_size))

    def across(self, q):
        return lax.rem(self.p + q, self.flat)

    def nearest(self, i):
        last = self.deep - 1
        span = jnp.minimum(self.a, last - self.a)
        zigzag = self.a + ((i + 1) // 2 if i % 2 else -(i // 2))
        return jnp.where(i <= 2 * span, zigzag, jnp.where(self.a < last - self.a, i, last - i))


def tiles_of(width, most=512):
    step = math.gcd(width, most)
    return [slice(i, i + step) for i in range(0, width, step)]


def flatten_rows(block):
    groups, rows, width = block.shape
    if rows % 16 == 0:
        return block.reshape(groups * rows, width)
    return block.astype(jnp.float32).reshape(groups * rows, width).astype(jnp.bfloat16)


def experts_kernel(
    sizes, x_ref, middle_ref, select_ref, mix_ref, gate_ref, up_ref, down_ref,
    wide_gate, wide_up, wide_down, out_ref,
    column_ref, stage_ref, arrived_ref, made_ref, back_ref, sent_ref, came_ref, base_ref,
    hidden_ref, own_gate, own_up, own_down,
    weight_sem, zs, zr, ps, pr, bs, br, ss, sr,
):
    at = Place(*sizes).here()
    last = at.deep - 1
    flat, rows = stage_ref.shape[1], stage_ref.shape[2]
    width = x_ref.shape[1]
    experts = own_gate.shape[0]
    cap = rows // experts
    loads = [
        pltpu.make_async_copy(wide_gate, own_gate, weight_sem.at[0]),
        pltpu.make_async_copy(wide_up, own_up, weight_sem.at[1]),
        pltpu.make_async_copy(wide_down, own_down, weight_sem.at[2]),
    ]
    for load in loads:
        load.start()
    has_right, has_left = at.a < last, at.a > 0
    greet(
        [at.column(lax.rem(at.a + d, at.deep)) for d in range(1, at.deep)]
        + [at.plane(at.across(q)) for q in range(1, flat)]
    )

    def relay(source, owner, side):
        return remote(
            source,
            column_ref.at[owner],
            zs.at[side, owner],
            zr.at[owner],
            at.column(at.a + (1 if side == 0 else -1)),
        )

    def sends(owner):
        right = has_right & (owner <= at.a)
        left = has_left & (owner >= at.a)
        return right, left

    def forward(source, owner):
        right, left = sends(owner)
        pl.when(right)(lambda: relay(source, owner, 0).start())
        pl.when(left)(lambda: relay(source, owner, 1).start())

    def out_copy(owner, q):
        target = at.across(q)
        return remote(
            stage_ref.at[owner, target],
            arrived_ref.at[owner, at.p],
            ps.at[owner, q],
            pr.at[owner, q],
            at.plane(target),
        )

    def back_copy(owner, q):
        target = at.across(q)
        return remote(
            made_ref.at[owner, target],
            back_ref.at[owner, at.p],
            bs.at[owner, q],
            br.at[owner, q],
            at.plane(target),
        )

    def pass_on(owner, source):
        for cut in tiles_of(width):
            picked = jnp.dot(
                select_ref[owner], source[:, cut], preferred_element_type=jnp.float32
            )
            stage_ref[owner, :, :, cut] = picked.reshape(flat, rows, -1).astype(jnp.bfloat16)
        for q in range(1, flat):
            out_copy(owner, q).start()
        arrived_ref[owner, at.p] = stage_ref[owner, at.p]

    def run_experts(owner):
        for q in range(1, flat):
            out_copy(owner, q).wait_recv()
        for e in range(experts):
            mine = slice(e * cap, (e + 1) * cap)
            for cut in tiles_of(own_gate.shape[2], 256):
                block = flatten_rows(arrived_ref[owner, :, mine, :])
                gate = jnp.dot(block, own_gate[e, :, cut], preferred_element_type=jnp.float32)
                up = jnp.dot(block, own_up[e, :, cut], preferred_element_type=jnp.float32)
                hidden_ref[:, cut] = (jax.nn.silu(gate) * up).astype(jnp.bfloat16)
            for cut in tiles_of(width):
                down = jnp.dot(
                    hidden_ref[...], own_down[e, :, cut], preferred_element_type=jnp.float32
                )
                made_ref[owner, :, mine, cut] = down.reshape(flat, cap, -1).astype(jnp.bfloat16)
        for q in range(1, flat):
            back_copy(owner, q).start()
        back_ref[owner, at.p] = made_ref[owner, at.p]

    order = [at.nearest(i) for i in range(at.deep)]
    forward(x_ref, at.a)
    pass_on(at.a, x_ref)
    tokens = x_ref.shape[0]
    for cut in tiles_of(gate_ref.shape[1], 256):
        gate = jnp.dot(x_ref[...], gate_ref[:, cut], preferred_element_type=jnp.float32)
        up = jnp.dot(x_ref[...], up_ref[:, cut], preferred_element_type=jnp.float32)
        sent_ref[at.a, :, cut] = (jax.nn.silu(gate) * up).astype(jnp.bfloat16)
    for cut in tiles_of(width):
        base_ref[:, cut] = middle_ref[:, cut].astype(jnp.float32) + jnp.dot(
            sent_ref[at.a, :, : gate_ref.shape[1]],
            down_ref[:, cut],
            preferred_element_type=jnp.float32,
        )
    for i in range(1, at.deep + 1):
        if i < at.deep:
            relay(x_ref, order[i], 0).wait_recv()
            forward(column_ref.at[order[i]], order[i])
            pass_on(order[i], column_ref.at[order[i]])
        if i == 1:
            for load in loads:
                load.wait()
        run_experts(order[i - 1])

    def gather_back(owner):
        for q in range(1, flat):
            back_copy(owner, q).wait_recv()

    def mixed(owner, cut):
        block = flatten_rows(back_ref[owner, :, :, cut])
        return jnp.dot(mix_ref[owner], block, preferred_element_type=jnp.float32)

    def toward(owner, side):
        return remote(
            sent_ref.at[owner],
            came_ref.at[side, owner],
            ss.at[owner],
            sr.at[side, owner],
            at.column(at.a + (-1 if side == 0 else 1)),
        )

    def step(owner, side, more):
        for cut in tiles_of(width):
            part = mixed(owner, cut)
            if more:
                part = part + came_ref[side, owner, :, cut].astype(jnp.float32)
            sent_ref[owner, :, cut] = part.astype(jnp.bfloat16)
        toward(owner, side).start()

    for i in range(at.deep - 1, 0, -1):
        owner = order[i]
        gather_back(owner)
        for side, goes, far in ((0, owner < at.a, has_right), (1, owner > at.a, has_left)):

            @pl.when(goes & far)
            def _(owner=owner, side=side):
                toward(owner, side).wait_recv()
                step(owner, side, True)

            @pl.when(goes & jnp.logical_not(far))
            def _(owner=owner, side=side):
                step(owner, side, False)

    gather_back(at.a)
    for cut in tiles_of(width):
        base_ref[:, cut] += mixed(at.a, cut)
    for side, far in ((0, has_right), (1, has_left)):

        @pl.when(far)
        def _(side=side):
            toward(at.a, side).wait_recv()
            for cut in tiles_of(width):
                base_ref[:, cut] += came_ref[side, at.a, :, cut].astype(jnp.float32)

    out_ref[...] = base_ref[...].astype(out_ref.dtype)
    for i in range(at.deep):
        owner = order[i]
        right, left = sends(owner)
        pl.when(right)(lambda owner=owner: relay(x_ref, owner, 0).wait_send())
        pl.when(left)(lambda owner=owner: relay(x_ref, owner, 1).wait_send())
        for q in range(1, flat):
            out_copy(owner, q).wait_send()
            back_copy(owner, q).wait_send()
        if i > 0:
            toward(owner, 0).wait_send()


def experts_layer(normed, middle, select, mix, common, routed):
    sizes = (lax.axis_size("sp"), lax.axis_size("tp"))
    at = Place(*sizes)
    tokens, width = normed.shape
    slots = select.shape[1]
    box = (at.deep, at.flat, slots // at.flat, width)
    chunk = (at.deep, tokens, width)
    dma = pltpu.SemaphoreType.DMA
    half = jnp.bfloat16
    vmem = pl.BlockSpec(memory_space=pltpu.VMEM)
    far = pl.BlockSpec(memory_space=pl.ANY)
    experts = routed[0].shape[0]
    return pl.pallas_call(
        functools.partial(experts_kernel, sizes),
        out_shape=jax.ShapeDtypeStruct((tokens, width), half),
        in_specs=[vmem] * 7 + [far] * 3,
        out_specs=vmem,
        scratch_shapes=[
            pltpu.VMEM(chunk, half),
            pltpu.VMEM(box, half),
            pltpu.VMEM(box, half),
            pltpu.VMEM(box, half),
            pltpu.VMEM(box, half),
            pltpu.VMEM(chunk, half),
            pltpu.VMEM((2,) + chunk, half),
            pltpu.VMEM((tokens, width), jnp.float32),
            pltpu.VMEM((slots // experts, routed[0].shape[2]), half),
            pltpu.VMEM(routed[0].shape, half),
            pltpu.VMEM(routed[1].shape, half),
            pltpu.VMEM(routed[2].shape, half),
            dma((3,)),
            dma((2, at.deep)),
            dma((at.deep,)),
            dma((at.deep, at.flat)),
            dma((at.deep, at.flat)),
            dma((at.deep, at.flat)),
            dma((at.deep, at.flat)),
            dma((at.deep,)),
            dma((2, at.deep)),
        ],
        compiler_params=pltpu.CompilerParams(
            collective_id=2, has_side_effects=True, vmem_limit_bytes=60 * 1024 * 1024
        ),
    )(normed, middle, select, mix, *common, *routed)


def on_device(
    queries,
    key_matrix,
    value_matrix,
    channel_decay_input,
    head_decay_offset,
    output_gate_input,
    head_norm_gain,
    residual,
    mixer_output_weight,
    expert_norm_gain,
    routes,
    chosen_router_scores,
    routed_gate_weight,
    routed_up_weight,
    routed_down_weight,
    common_gate_weight,
    common_up_weight,
    common_down_weight,
):
    device_heads = head_decay_offset.shape[1]
    seq_rows = queries.shape[0]
    blocks = seq_rows // BLOCK

    def split_local(values, columns):
        return (
            values.astype(jnp.float32)
            .reshape(blocks, BLOCK, device_heads, columns)
            .transpose(2, 0, 1, 3)
        )

    decay_spike_columns = jnp.repeat(head_decay_offset, KEY_CHANNELS, axis=1)
    decay_logarithm = (
        jax.nn.log_sigmoid(channel_decay_input.astype(jnp.float32)) / decay_running
        + decay_spike_columns
    )
    within = jnp.einsum(
        "ij,hnjd->hnid",
        jnp.tril(jnp.ones((BLOCK, BLOCK), jnp.float32)),
        split_local(decay_logarithm, KEY_CHANNELS),
        precision=lax.Precision.HIGHEST,
    )
    block_end = within[:, :, -1, :]
    q_heads = split_local(queries, KEY_CHANNELS) * KEY_CHANNELS ** (-0.5)
    k_heads = split_local(key_matrix, KEY_CHANNELS)
    v_heads = split_local(value_matrix, VDIM)
    q_decay = q_heads * jnp.exp(within)
    k_grow = k_heads * jnp.exp(-within)
    k_tail = k_heads * jnp.exp(block_end[:, :, None, :] - within)
    causal = jnp.tril(jnp.ones((BLOCK, BLOCK), dtype=bool))
    scores = jnp.where(causal, jnp.einsum("hnid,hnjd->hnij", q_decay, k_grow), 0.0)
    inside = jnp.einsum("hnij,hnje->hnie", scores, v_heads)
    block_state = jnp.einsum("hncd,hnce->hnde", k_tail, v_heads)
    inclusive = jnp.cumsum(block_end, axis=1)
    exclusive = inclusive - block_end
    before = jnp.arange(blocks)[:, None] > jnp.arange(blocks)[None, :]
    spread = jnp.exp(
        jnp.where(
            before[None, :, :, None], exclusive[:, :, None, :] - inclusive[:, None, :, :], -jnp.inf
        )
    )
    local_start = jnp.einsum("hnmd,hmde->hnde", spread, block_state)
    total_log = inclusive[:, -1, :]
    tail_weight = jnp.exp(total_log[:, None, :] - inclusive)
    device_state = jnp.einsum("hnd,hnde->hde", tail_weight, block_state)
    lanes = VDIM
    tok_count = residual.shape[0]
    sp_index = lax.axis_index("sp")
    sp_size = lax.axis_size("sp")
    state_rows = device_heads * KEY_CHANNELS
    parts = [
        total_log.reshape(-1, lanes),
        routes.T.astype(jnp.float32).reshape(-1, lanes),
        chosen_router_scores.T.reshape(-1, lanes),
    ]
    stops = [sum(part.shape[0] for part in parts[: i + 1]) for i in range(len(parts))]
    spare = -stops[-1] % 8
    packet = jnp.concatenate(parts + [jnp.zeros((spare, lanes), jnp.float32)], axis=0)
    state = device_state.reshape(state_rows, lanes).astype(jnp.bfloat16)
    states, gathered = gather_sp(state, packet)
    states = states.reshape(sp_size, device_heads, KEY_CHANNELS, VDIM).astype(jnp.float32)
    logs = gathered[:, : stops[0]].reshape(sp_size, device_heads, KEY_CHANNELS)
    ahead = (jnp.arange(sp_size) < sp_index)[:, None, None]
    logs = jnp.where(ahead, logs, 0.0)
    later = (jnp.arange(sp_size)[:, None] < jnp.arange(sp_size)[None, :])[:, :, None, None]
    after = jnp.sum(jnp.where(later, logs[None], 0.0), axis=1)
    reach = jnp.where(ahead, jnp.exp(after), 0.0)
    carried = jnp.sum(reach[..., None] * states, axis=0)
    entering = local_start + jnp.exp(exclusive)[..., None] * carried[:, None, :, :]
    output = inside + jnp.einsum("hncd,hnde->hnce", q_decay, entering)
    output = output.transpose(1, 2, 0, 3).reshape(seq_rows, device_heads, VDIM)
    inv_rms = lax.rsqrt(jnp.mean(output * output, axis=-1, keepdims=True) + eps_norm)
    normed_heads = (output * inv_rms * head_norm_gain).reshape(seq_rows, device_heads * VDIM)
    gated_output = (normed_heads * jax.nn.silu(output_gate_input.astype(jnp.float32))).astype(
        jnp.bfloat16
    )
    stacked = gated_output.reshape(lax.axis_size("tp"), tok_count, gated_output.shape[1])
    projected = jnp.dot(
        swap_tp(stacked), mixer_output_weight, preferred_element_type=jnp.float32
    )
    middle = (residual.astype(jnp.float32) + projected).astype(jnp.bfloat16)
    middle_wide = middle.astype(jnp.float32)
    norm_scale = lax.rsqrt(jnp.mean(middle_wide * middle_wide, axis=-1, keepdims=True) + eps_norm)
    normed = (middle_wide * norm_scale * expert_norm_gain).astype(jnp.bfloat16)
    devices = sp_size * lax.axis_size("tp")
    exp_dev = routed_gate_weight.shape[0]
    cap_slots = 2 * TOP_K * tok_count // (exp_dev * devices)
    at = Place(sp_size, lax.axis_size("tp")).here()
    column = lax.dynamic_index_in_dim(
        gathered.reshape(at.deep, at.rows, -1, lanes), at.b, 1, False
    )
    names = column[:, stops[0] : stops[1]].reshape(at.deep, TOP_K, 1, tok_count)
    scores_all = column[:, stops[1] : stops[2]].reshape(at.deep, TOP_K, 1, tok_count)
    weights = routed_scale * scores_all / jnp.sum(scores_all, axis=1, keepdims=True)
    plane_experts = at.flat * exp_dev
    expert = (at.a * plane_experts + jnp.arange(plane_experts)).astype(jnp.float32)
    hit = (names == expert[None, None, :, None]).astype(jnp.float32)
    chosen = jnp.sum(hit, axis=1)
    weight_of = jnp.sum(hit * weights, axis=1)
    sooner = jnp.triu(jnp.ones((tok_count, tok_count), jnp.bfloat16), 1)
    rank = jnp.einsum(
        "aeu,ut->aet",
        chosen.astype(jnp.bfloat16),
        sooner,
        preferred_element_type=jnp.float32,
    )
    slot = jnp.arange(cap_slots, dtype=jnp.float32)[None, None, :, None]
    taken = (rank[:, :, None, :] == slot) & (chosen[:, :, None, :] > 0.0)
    slots = plane_experts * cap_slots
    select = taken.astype(jnp.bfloat16).reshape(at.deep, slots, tok_count)
    mix = jnp.where(taken, weight_of[:, :, None, :], 0.0).astype(jnp.bfloat16)
    mix = mix.reshape(at.deep, slots, tok_count).transpose(0, 2, 1)
    return experts_layer(
        normed,
        middle,
        select,
        mix,
        (common_gate_weight, common_up_weight, common_down_weight),
        (routed_gate_weight, routed_up_weight, routed_down_weight),
    )


def solution(mesh):
    placed = (
        P("sp", "tp"),
        P("sp", "tp"),
        P("sp", "tp"),
        P("sp", "tp"),
        P("sp", "tp"),
        P("sp", "tp"),
        P(),
        P(("sp", "tp"), None),
        P(),
        P(),
        P(("sp", "tp"), None),
        P(("sp", "tp"), None),
        P(("sp", "tp"), None, None),
        P(("sp", "tp"), None, None),
        P(("sp", "tp"), None, None),
        P(),
        P(),
        P(),
    )
    return jax.shard_map(
        on_device, mesh=mesh, in_specs=placed, out_specs=P(("sp", "tp"), None), check_vma=False
    )
```

profile of v0, /device:TPU:18, one launch (start us, length us, event | category | flops | bytes accessed | tf_op | source)
XLA Modules:
  0.0 181.4 jit_solution(575246202555431783)
XLA Ops:
  0.0 0.0 copy-start
  0.0 1.1 copy.60
  1.1 0.9 fusion.34
  1.9 0.1 reshape.149
  2.1 0.2 copy.61
  2.3 0.0 copy-start.8
  2.3 0.0 copy-start.9
  2.3 0.6 convolution_bitcast_fusion
  3.0 1.2 reshape.162
  4.2 0.0 copy-done.5
  4.2 0.3 reshape.161
  4.6 0.0 copy-done.3
  4.6 0.1 reshape.151
  4.7 0.4 fusion.2
  5.1 0.3 fusion.12
  5.3 0.0 copy-start.4
  5.4 0.1 copy.80
  5.6 0.3 fusion.28
  5.9 0.6 convert_element_type.65
  6.5 0.0 copy-done.8
  6.5 0.1 reshape_squeeze.3
  6.6 0.1 pad.3.clone
  6.7 0.0 copy-done.9
  6.7 0.7 maximum_maximum_fusion.y_ref
  7.3 11.3 %shard_map.172 = (bf16[8,128,128]{2,1,0:T(8,128)(2,1)}, f32[8,16,128]{2,1,0:T(8,128)}) custom-call(bf16[128,128]{1,0:T(8,128)(2,1)} %bitcast.95, f32[16,128]{1,0:T(8,128)} %maximum_maximum_fusion.y_ref), custom_call_target="tpu_custom_call" | custom-call | tf_op jit(solution)/shard_map/pallas_call | solution.py:50
  18.6 0.8 slice_reduce_fusion
  19.4 0.1 reshape.152
  19.5 0.1 broadcast_select_fusion
  19.6 0.1 select_reduce_fusion
  19.7 0.1 exp.49
  19.8 0.1 broadcast_select_fusion.1
  19.9 1.2 multiply_reduce_fusion.1
  21.0 0.1 copy.69
  21.1 0.1 copy.67
  21.2 0.1 copy.66
  21.4 0.0 copy-start.2
  21.4 0.4 fusion.3
  21.8 0.4 multiply_reduce_fusion
  22.2 0.1 copy.86
  22.4 0.6 mul.131
  23.0 0.0 copy-start.7
  23.0 0.4 copy.72
  23.4 0.0 copy-done
  23.4 0.0 copy-done.4
  23.4 0.0 copy-start.6
  23.4 0.9 fusion.24
  24.3 6.7 %shard_map.173 = bf16[128,1024]{1,0:T(8,128)(2,1)} custom-call(bf16[4,128,256]{2,1,0:T(8,128)(2,1)} %bitcast.89), custom_call_target="tpu_custom_call" | custom-call | tf_op jit(solution)/shard_map/pallas_call | solution.py:50
  31.0 0.0 copy-done.2
  31.0 3.2 %fusion.4 = (f32[128]{0:T(128)S(1)}, bf16[128,2048]{1,0:T(8,128)(2,1)S(1)}) fusion(bf16[128,1024]{1,0:T(8,128)(2,1)} %shard_map.173, bf16[1024,2048]{1,0:T(8,128)(2,1)} %param.26, bf16[128,2048]{1,0:T(8,128)(2,1)S(1)} %copy-done.2), kind=kOutput, calls=%fused_computation.11 | convolution fusion | flops 538443648 | bytes 5505536 | tf_op jit(solution)/shard_map/dot_general | solution.py:494
  34.2 0.0 copy-start.1
  34.2 0.0 copy-done.7
  34.2 1.0 fusion.6.x_ref
  35.2 0.0 copy-done.6
  35.3 0.1 fusion.47
  35.4 0.1 copy.76
  35.6 0.3 copy.75
  35.9 0.1 fusion.50
  36.1 0.2 copy.74
  36.3 0.1 eq.40
  36.4 0.9 fusion.31
  37.3 0.9 copy.77.select_ref
  38.2 0.0 copy-done.1
  38.2 141.3 %shard_map.174 = bf16[128,2048]{1,0:T(8,128)(2,1)} custom-call(bf16[128,2048]{1,0:T(8,128)(2,1)} %fusion.6.x_ref, bf16[128,2048]{1,0:T(8,128)(2,1)} %copy-done.1, bf16[4,256,128]{2,1,0:T(8,128)(2,1)} %copy.77.select_ref, bf16[4,128,256]{2,1,0:T(8,128)(2,1)} %get-tuple-element.11.mix_ref, bf16[2048,512]{1,0:T(8,128)(2,1)} %gate_ref.1, ...), custom_call_target="tpu_custom_call" | custom-call | tf_op jit(solution)/shard_map/pallas_call | solution.py:363
  179.5 1.9 %copy.127 = bf16[128,2048]{1,0:T(8,128)(2,1)} copy(bf16[128,2048]{1,0:T(8,128)(2,1)} %shard_map.174) | data formatting | bytes 1048576
  (30 shorter events, 0.4 us)
Async XLA Ops:
  0.0 23.4 %copy-start = (f32[128]{0:T(128)S(1)}, f32[128]{0:T(128)}, u32[]{:S(2)}) copy-start(f32[128]{0:T(128)} %param.24) | copy-start | bytes 1540
  0.0 4.2 %copy-start.5 = (bf16[512,128]{1,0:T(8,128)(2,1)S(1)}, bf16[512,128]{1,0:T(8,128)(2,1)}, u32[]{:S(2)}) copy-start(bf16[512,128]{1,0:T(8,128)(2,1)} %param.18) | copy-start | bytes 393220
  0.0 4.6 %copy-start.3 = (bf16[512,256]{1,0:T(8,128)(2,1)S(1)}, bf16[512,256]{1,0:T(8,128)(2,1)}, u32[]{:S(2)}) copy-start(bf16[512,256]{1,0:T(8,128)(2,1)} %param.20) | copy-start | bytes 786436
  2.3 4.2 %copy-start.8 = (s32[128,4]{0,1:T(4,128)S(1)}, s32[128,4]{0,1:T(4,128)}, u32[]{:S(2)}) copy-start(s32[128,4]{0,1:T(4,128)} %param.28) | copy-start | bytes 6148
  2.3 4.3 %copy-start.9 = (f32[128,4]{0,1:T(4,128)S(1)}, f32[128,4]{0,1:T(4,128)}, u32[]{:S(2)}) copy-start(f32[128,4]{0,1:T(4,128)} %param.29) | copy-start | bytes 6148
  5.3 18.1 %copy-start.4 = (bf16[512,256]{1,0:T(8,128)(2,1)S(1)}, bf16[512,256]{1,0:T(8,128)(2,1)}, u32[]{:S(2)}) copy-start(bf16[512,256]{1,0:T(8,128)(2,1)} %param.23) | copy-start | bytes 786436
  21.4 9.6 %copy-start.2 = (bf16[128,2048]{1,0:T(8,128)(2,1)S(1)}, bf16[128,2048]{1,0:T(8,128)(2,1)}, u32[]{:S(2)}) copy-start(bf16[128,2048]{1,0:T(8,128)(2,1)} %param.25) | copy-start | bytes 1572868
  23.0 11.3 %copy-start.7 = (f32[2048]{0:T(1024)S(1)}, f32[2048]{0:T(1024)}, u32[]{:S(2)}) copy-start(f32[2048]{0:T(1024)} %param.27) | copy-start | bytes 24580
  23.4 11.8 %copy-start.6 = (f32[8,16,128]{2,1,0:T(8,128)S(1)}, f32[8,16,128]{2,1,0:T(8,128)}, u32[]{:S(2)}) copy-start(f32[8,16,128]{2,1,0:T(8,128)} %get-tuple-element.7) | copy-start | bytes 196612
  34.2 4.0 %copy-start.1 = (bf16[128,2048]{1,0:T(8,128)(2,1)}, bf16[128,2048]{1,0:T(8,128)(2,1)S(1)}, u32[]{:S(2)}) copy-start(bf16[128,2048]{1,0:T(8,128)(2,1)S(1)} %get-tuple-element.20.middle_ref) | copy-start | bytes 1572868
where the time goes:
time: 184 us; the launch traced here: 181 us
  Pallas kernels  159 us (86%)
  local copies, waits for them, and re-layouts  9.33 us (5%)
  other arithmetic  6.62 us (4%)
  matrix products  5.71 us (3%)
    pallas_call x1, Pallas kernels, experts_layer(): pl.pallas_call(functools.partial(experts_kernel, sizes), out_shape=jax.Sh...  141 us
    pallas_call x2, Pallas kernels, remote_call(): pl.pallas_call(kernel, out_shape=out_shape, in_specs=[vmem] * len(operand...  18 us

commit v1 on v0

--- a/solution.py
+++ b/solution.py
@@ -171,7 +171,7 @@
     sizes, x_ref, middle_ref, select_ref, mix_ref, gate_ref, up_ref, down_ref,
     wide_gate, wide_up, wide_down, out_ref,
     column_ref, stage_ref, arrived_ref, made_ref, back_ref, sent_ref, came_ref, base_ref,
-    hidden_ref, own_gate, own_up, own_down,
+    hidden_ref, shared_ref, own_gate, own_up, own_down,
     weight_sem, zs, zr, ps, pr, bs, br, ss, sr,
 ):
     at = Place(*sizes).here()
@@ -180,6 +180,7 @@
     width = x_ref.shape[1]
     experts = own_gate.shape[0]
     cap = rows // experts
+    cuts = tiles_of(width)
     loads = [
         pltpu.make_async_copy(wide_gate, own_gate, weight_sem.at[0]),
         pltpu.make_async_copy(wide_up, own_up, weight_sem.at[1]),
@@ -222,18 +223,18 @@
             at.plane(target),
         )
 
-    def back_copy(owner, q):
+    def back_copy(owner, q, i):
         target = at.across(q)
         return remote(
-            made_ref.at[owner, target],
-            back_ref.at[owner, at.p],
-            bs.at[owner, q],
-            br.at[owner, q],
+            made_ref.at[owner, target, :, cuts[i]],
+            back_ref.at[owner, at.p, :, cuts[i]],
+            bs.at[owner, q, i],
+            br.at[owner, q, i],
             at.plane(target),
         )
 
     def pass_on(owner, source):
-        for cut in tiles_of(width):
+        for cut in cuts:
             picked = jnp.dot(
                 select_ref[owner], source[:, cut], preferred_element_type=jnp.float32
             )
@@ -242,100 +243,104 @@
             out_copy(owner, q).start()
         arrived_ref[owner, at.p] = stage_ref[owner, at.p]
 
-    def run_experts(owner):
+    def send_back(owner, i):
+        for q in range(1, flat):
+            back_copy(owner, q, i).start()
+
+    def run_experts(owner, hold=False):
         for q in range(1, flat):
             out_copy(owner, q).wait_recv()
         for e in range(experts):
             mine = slice(e * cap, (e + 1) * cap)
+            block = flatten_rows(arrived_ref[owner, :, mine, :])
             for cut in tiles_of(own_gate.shape[2], 256):
-                block = flatten_rows(arrived_ref[owner, :, mine, :])
                 gate = jnp.dot(block, own_gate[e, :, cut], preferred_element_type=jnp.float32)
                 up = jnp.dot(block, own_up[e, :, cut], preferred_element_type=jnp.float32)
-                hidden_ref[:, cut] = (jax.nn.silu(gate) * up).astype(jnp.bfloat16)
-            for cut in tiles_of(width):
+                hidden_ref[e, :, cut] = (jax.nn.silu(gate) * up).astype(jnp.bfloat16)
+        for i, cut in enumerate(cuts):
+            for e in range(experts):
+                mine = slice(e * cap, (e + 1) * cap)
                 down = jnp.dot(
-                    hidden_ref[...], own_down[e, :, cut], preferred_element_type=jnp.float32
+                    hidden_ref[e], own_down[e, :, cut], preferred_element_type=jnp.float32
                 )
                 made_ref[owner, :, mine, cut] = down.reshape(flat, cap, -1).astype(jnp.bfloat16)
+            if not hold:
+                send_back(owner, i)
+        back_ref[owner, at.p] = made_ref[owner, at.p]
+
+    def mixed(owner, i):
         for q in range(1, flat):
-            back_copy(owner, q).start()
-        back_ref[owner, at.p] = made_ref[owner, at.p]
+            back_copy(owner, q, i).wait_recv()
+        block = flatten_rows(back_ref[owner, :, :, cuts[i]])
+        return jnp.dot(mix_ref[owner], block, preferred_element_type=jnp.float32)
+
+    def toward(owner, side, i):
+        return remote(
+            sent_ref.at[owner, :, cuts[i]],
+            came_ref.at[side, owner, :, cuts[i]],
+            ss.at[owner, i],
+            sr.at[side, owner, i],
+            at.column(at.a + (-1 if side == 0 else 1)),
+        )
+
+    def step(owner, side, more):
+        for i, cut in enumerate(cuts):
+            part = mixed(owner, i)
+            if more:
+                toward(owner, side, i).wait_recv()
+                part = part + came_ref[side, owner, :, cut].astype(jnp.float32)
+            sent_ref[owner, :, cut] = part.astype(jnp.bfloat16)
+            toward(owner, side, i).start()
+
+    def homeward(turn):
+        for owner, side, far in ((last - turn, 0, has_right), (turn, 1, has_left)):
+            goes = (owner < at.a) if side == 0 else (owner > at.a)
+            pl.when(goes & far)(lambda owner=owner, side=side: step(owner, side, True))
+            pl.when(goes & jnp.logical_not(far))(
+                lambda owner=owner, side=side: step(owner, side, False)
+            )
+
+    def take(i):
+        relay(x_ref, order[i], 0).wait_recv()
+        forward(column_ref.at[order[i]], order[i])
+        pass_on(order[i], column_ref.at[order[i]])
 
     order = [at.nearest(i) for i in range(at.deep)]
     forward(x_ref, at.a)
     pass_on(at.a, x_ref)
-    tokens = x_ref.shape[0]
     for cut in tiles_of(gate_ref.shape[1], 256):
         gate = jnp.dot(x_ref[...], gate_ref[:, cut], preferred_element_type=jnp.float32)
         up = jnp.dot(x_ref[...], up_ref[:, cut], preferred_element_type=jnp.float32)
-        sent_ref[at.a, :, cut] = (jax.nn.silu(gate) * up).astype(jnp.bfloat16)
-    for cut in tiles_of(width):
+        shared_ref[:, cut] = (jax.nn.silu(gate) * up).astype(jnp.bfloat16)
+    for cut in cuts:
         base_ref[:, cut] = middle_ref[:, cut].astype(jnp.float32) + jnp.dot(
-            sent_ref[at.a, :, : gate_ref.shape[1]],
-            down_ref[:, cut],
-            preferred_element_type=jnp.float32,
+            shared_ref[...], down_ref[:, cut], preferred_element_type=jnp.float32
         )
     for i in range(1, at.deep + 1):
         if i < at.deep:
-            relay(x_ref, order[i], 0).wait_recv()
-            forward(column_ref.at[order[i]], order[i])
-            pass_on(order[i], column_ref.at[order[i]])
+            take(i)
         if i == 1:
             for load in loads:
                 load.wait()
-        run_experts(order[i - 1])
-
-    def gather_back(owner):
-        for q in range(1, flat):
-            back_copy(owner, q).wait_recv()
-
-    def mixed(owner, cut):
-        block = flatten_rows(back_ref[owner, :, :, cut])
-        return jnp.dot(mix_ref[owner], block, preferred_element_type=jnp.float32)
-
-    def toward(owner, side):
-        return remote(
-            sent_ref.at[owner],
-            came_ref.at[side, owner],
-            ss.at[owner],
-            sr.at[side, owner],
-            at.column(at.a + (-1 if side == 0 else 1)),
-        )
-
-    def step(owner, side, more):
-        for cut in tiles_of(width):
-            part = mixed(owner, cut)
-            if more:
-                part = part + came_ref[side, owner, :, cut].astype(jnp.float32)
-            sent_ref[owner, :, cut] = part.astype(jnp.bfloat16)
-        toward(owner, side).start()
-
-    for i in range(at.deep - 1, 0, -1):
-        owner = order[i]
-        gather_back(owner)
-        for side, goes, far in ((0, owner < at.a, has_right), (1, owner > at.a, has_left)):
-
-            @pl.when(goes & far)
-            def _(owner=owner, side=side):
-                toward(owner, side).wait_recv()
-                step(owner, side, True)
-
-            @pl.when(goes & jnp.logical_not(far))
-            def _(owner=owner, side=side):
-                step(owner, side, False)
-
-    gather_back(at.a)
-    for cut in tiles_of(width):
-        base_ref[:, cut] += mixed(at.a, cut)
+        if i == at.deep:
+            for turn in range(1, at.deep - 2):
+                homeward(turn)
+        run_experts(order[i - 1], hold=i == 1)
+    for i in range(len(cuts)):
+        send_back(at.a, i)
+    for turn in range(max(1, at.deep - 2), at.deep):
+        homeward(turn)
+
     for side, far in ((0, has_right), (1, has_left)):
 
         @pl.when(far)
         def _(side=side):
-            toward(at.a, side).wait_recv()
-            for cut in tiles_of(width):
+            for i, cut in enumerate(cuts):
+                toward(at.a, side, i).wait_recv()
                 base_ref[:, cut] += came_ref[side, at.a, :, cut].astype(jnp.float32)
 
-    out_ref[...] = base_ref[...].astype(out_ref.dtype)
+    for i, cut in enumerate(cuts):
+        out_ref[:, cut] = (base_ref[:, cut] + mixed(at.a, i)).astype(out_ref.dtype)
     for i in range(at.deep):
         owner = order[i]
         right, left = sends(owner)
@@ -343,9 +348,11 @@
         pl.when(left)(lambda owner=owner: relay(x_ref, owner, 1).wait_send())
         for q in range(1, flat):
             out_copy(owner, q).wait_send()
-            back_copy(owner, q).wait_send()
+            for j in range(len(cuts)):
+                back_copy(owner, q, j).wait_send()
         if i > 0:
-            toward(owner, 0).wait_send()
+            for j in range(len(cuts)):
+                toward(owner, 0, j).wait_send()
 
 
 def experts_layer(normed, middle, select, mix, common, routed):
@@ -360,6 +367,7 @@
     vmem = pl.BlockSpec(memory_space=pltpu.VMEM)
     far = pl.BlockSpec(memory_space=pl.ANY)
     experts = routed[0].shape[0]
+    parts = len(tiles_of(width))
     return pl.pallas_call(
         functools.partial(experts_kernel, sizes),
         out_shape=jax.ShapeDtypeStruct((tokens, width), half),
@@ -374,7 +382,8 @@
             pltpu.VMEM(chunk, half),
             pltpu.VMEM((2,) + chunk, half),
             pltpu.VMEM((tokens, width), jnp.float32),
-            pltpu.VMEM((slots // experts, routed[0].shape[2]), half),
+            pltpu.VMEM((experts, slots // experts, routed[0].shape[2]), half),
+            pltpu.VMEM((tokens, common[0].shape[1]), half),
             pltpu.VMEM(routed[0].shape, half),
             pltpu.VMEM(routed[1].shape, half),
             pltpu.VMEM(routed[2].shape, half),
@@ -383,10 +392,10 @@
             dma((at.deep,)),
             dma((at.deep, at.flat)),
             dma((at.deep, at.flat)),
-            dma((at.deep, at.flat)),
-            dma((at.deep, at.flat)),
-            dma((at.deep,)),
-            dma((2, at.deep)),
+            dma((at.deep, at.flat, parts)),
+            dma((at.deep, at.flat, parts)),
+            dma((at.deep, parts)),
+            dma((2, at.deep, parts)),
         ],
         compiler_params=pltpu.CompilerParams(
             collective_id=2, has_side_effects=True, vmem_limit_bytes=60 * 1024 * 1024

time: 184 us -> 169 us (0.918)
  Pallas kernels: 159 us -> 144 us
    pallas_call x1, Pallas kernels: 141 us -> 126 us  [experts_layer(): pl.pallas_call(functools.partial(experts_kernel, sizes), out_shape=jax.Sh...]
where the time goes in v1:
time: 169 us; the launch traced here: 166 us
  Pallas kernels  144 us (85%)
  local copies, waits for them, and re-layouts  9.33 us (6%)
  other arithmetic  6.62 us (4%)
  matrix products  5.71 us (3%)
    pallas_call x1, Pallas kernels, experts_layer(): pl.pallas_call(functools.partial(experts_kernel, sizes), out_shape=jax.Sh...  126 us
    pallas_call x2, Pallas kernels, remote_call(): pl.pallas_call(kernel, out_shape=out_shape, in_specs=[vmem] * len(operand...  18 us

profile of v1, /device:TPU:18, one launch (start us, length us, event | category | flops | bytes accessed | tf_op | source)
XLA Modules:
  0.0 166.4 jit_solution(2772103673800385914)
XLA Ops:
  0.0 0.0 copy-start
  0.0 1.1 copy.60
  1.1 0.9 fusion.34
  1.9 0.1 reshape.149
  2.1 0.2 copy.61
  2.3 0.0 copy-start.8
  2.3 0.0 copy-start.9
  2.3 0.6 convolution_bitcast_fusion
  3.0 1.2 reshape.162
  4.2 0.0 copy-done.5
  4.2 0.3 reshape.161
  4.6 0.0 copy-done.3
  4.6 0.1 reshape.151
  4.7 0.4 fusion.2
  5.1 0.3 fusion.12
  5.3 0.0 copy-start.4
  5.4 0.1 copy.80
  5.6 0.3 fusion.28
  5.9 0.6 convert_element_type.65
  6.5 0.0 copy-done.8
  6.5 0.1 reshape_squeeze.3
  6.6 0.1 pad.3.clone
  6.7 0.0 copy-done.9
  6.7 0.7 maximum_maximum_fusion.y_ref
  7.3 11.3 %shard_map.172 = (bf16[8,128,128]{2,1,0:T(8,128)(2,1)}, f32[8,16,128]{2,1,0:T(8,128)}) custom-call(bf16[128,128]{1,0:T(8,128)(2,1)} %bitcast.95, f32[16,128]{1,0:T(8,128)} %maximum_maximum_fusion.y_ref), custom_call_target="tpu_custom_call" | custom-call | tf_op jit(solution)/shard_map/pallas_call | solution.py:50
  18.6 0.8 slice_reduce_fusion
  19.4 0.1 reshape.152
  19.5 0.1 broadcast_select_fusion
  19.6 0.1 select_reduce_fusion
  19.7 0.1 exp.49
  19.8 0.1 broadcast_select_fusion.1
  19.9 1.2 multiply_reduce_fusion.1
  21.0 0.1 copy.69
  21.1 0.1 copy.67
  21.2 0.1 copy.66
  21.4 0.0 copy-start.2
  21.4 0.4 fusion.3
  21.8 0.4 multiply_reduce_fusion
  22.2 0.1 copy.86
  22.4 0.6 mul.131
  23.0 0.0 copy-start.7
  23.0 0.4 copy.72
  23.4 0.0 copy-done
  23.4 0.0 copy-done.4
  23.4 0.0 copy-start.6
  23.4 0.9 fusion.24
  24.3 6.7 %shard_map.173 = bf16[128,1024]{1,0:T(8,128)(2,1)} custom-call(bf16[4,128,256]{2,1,0:T(8,128)(2,1)} %bitcast.89), custom_call_target="tpu_custom_call" | custom-call | tf_op jit(solution)/shard_map/pallas_call | solution.py:50
  31.0 0.0 copy-done.2
  31.0 3.2 %fusion.4 = (f32[128]{0:T(128)S(1)}, bf16[128,2048]{1,0:T(8,128)(2,1)S(1)}) fusion(bf16[128,1024]{1,0:T(8,128)(2,1)} %shard_map.173, bf16[1024,2048]{1,0:T(8,128)(2,1)} %param.26, bf16[128,2048]{1,0:T(8,128)(2,1)S(1)} %copy-done.2), kind=kOutput, calls=%fused_computation.11 | convolution fusion | flops 538443648 | bytes 5505536 | tf_op jit(solution)/shard_map/dot_general | solution.py:503
  34.2 0.0 copy-start.1
  34.2 0.0 copy-done.7
  34.2 1.0 fusion.6.x_ref
  35.2 0.0 copy-done.6
  35.3 0.1 fusion.47
  35.4 0.1 copy.76
  35.6 0.3 copy.75
  35.9 0.1 fusion.50
  36.1 0.2 copy.74
  36.3 0.1 eq.40
  36.4 0.9 fusion.31
  37.3 0.9 copy.77.select_ref
  38.2 0.0 copy-done.1
  38.2 126.4 %shard_map.174 = bf16[128,2048]{1,0:T(8,128)(2,1)} custom-call(bf16[128,2048]{1,0:T(8,128)(2,1)} %fusion.6.x_ref, bf16[128,2048]{1,0:T(8,128)(2,1)} %copy-done.1, bf16[4,256,128]{2,1,0:T(8,128)(2,1)} %copy.77.select_ref, bf16[4,128,256]{2,1,0:T(8,128)(2,1)} %get-tuple-element.11.mix_ref, bf16[2048,512]{1,0:T(8,128)(2,1)} %gate_ref.1, ...), custom_call_target="tpu_custom_call" | custom-call | tf_op jit(solution)/shard_map/pallas_call | solution.py:371
  164.6 1.9 %copy.127 = bf16[128,2048]{1,0:T(8,128)(2,1)} copy(bf16[128,2048]{1,0:T(8,128)(2,1)} %shard_map.174) | data formatting | bytes 1048576
  (30 shorter events, 0.4 us)
Async XLA Ops:
  0.0 23.4 %copy-start = (f32[128]{0:T(128)S(1)}, f32[128]{0:T(128)}, u32[]{:S(2)}) copy-start(f32[128]{0:T(128)} %param.24) | copy-start | bytes 1540
  0.0 4.2 %copy-start.5 = (bf16[512,128]{1,0:T(8,128)(2,1)S(1)}, bf16[512,128]{1,0:T(8,128)(2,1)}, u32[]{:S(2)}) copy-start(bf16[512,128]{1,0:T(8,128)(2,1)} %param.18) | copy-start | bytes 393220
  0.0 4.6 %copy-start.3 = (bf16[512,256]{1,0:T(8,128)(2,1)S(1)}, bf16[512,256]{1,0:T(8,128)(2,1)}, u32[]{:S(2)}) copy-start(bf16[512,256]{1,0:T(8,128)(2,1)} %param.20) | copy-start | bytes 786436
  2.3 4.2 %copy-start.8 = (s32[128,4]{0,1:T(4,128)S(1)}, s32[128,4]{0,1:T(4,128)}, u32[]{:S(2)}) copy-start(s32[128,4]{0,1:T(4,128)} %param.28) | copy-start | bytes 6148
  2.3 4.3 %copy-start.9 = (f32[128,4]{0,1:T(4,128)S(1)}, f32[128,4]{0,1:T(4,128)}, u32[]{:S(2)}) copy-start(f32[128,4]{0,1:T(4,128)} %param.29) | copy-start | bytes 6148
  5.3 18.1 %copy-start.4 = (bf16[512,256]{1,0:T(8,128)(2,1)S(1)}, bf16[512,256]{1,0:T(8,128)(2,1)}, u32[]{:S(2)}) copy-start(bf16[512,256]{1,0:T(8,128)(2,1)} %param.23) | copy-start | bytes 786436
  21.4 9.6 %copy-start.2 = (bf16[128,2048]{1,0:T(8,128)(2,1)S(1)}, bf16[128,2048]{1,0:T(8,128)(2,1)}, u32[]{:S(2)}) copy-start(bf16[128,2048]{1,0:T(8,128)(2,1)} %param.25) | copy-start | bytes 1572868
  23.0 11.3 %copy-start.7 = (f32[2048]{0:T(1024)S(1)}, f32[2048]{0:T(1024)}, u32[]{:S(2)}) copy-start(f32[2048]{0:T(1024)} %param.27) | copy-start | bytes 24580
  23.4 11.8 %copy-start.6 = (f32[8,16,128]{2,1,0:T(8,128)S(1)}, f32[8,16,128]{2,1,0:T(8,128)}, u32[]{:S(2)}) copy-start(f32[8,16,128]{2,1,0:T(8,128)} %get-tuple-element.7) | copy-start | bytes 196612
  34.2 4.0 %copy-start.1 = (bf16[128,2048]{1,0:T(8,128)(2,1)}, bf16[128,2048]{1,0:T(8,128)(2,1)S(1)}, u32[]{:S(2)}) copy-start(bf16[128,2048]{1,0:T(8,128)(2,1)S(1)} %get-tuple-element.20.middle_ref) | copy-start | bytes 1572868

commit v2 on v1

--- a/solution.py
+++ b/solution.py
@@ -168,10 +168,10 @@
 
 
 def experts_kernel(
-    sizes, x_ref, middle_ref, select_ref, mix_ref, gate_ref, up_ref, down_ref,
+    sizes, x_ref, middle_ref, select_ref, mix_ref, far_gate, far_up, far_down,
     wide_gate, wide_up, wide_down, out_ref,
     column_ref, stage_ref, arrived_ref, made_ref, back_ref, sent_ref, came_ref, base_ref,
-    hidden_ref, shared_ref, own_gate, own_up, own_down,
+    hidden_ref, shared_ref, gate_ref, up_ref, down_ref, own_gate, own_up, own_down,
     weight_sem, zs, zr, ps, pr, bs, br, ss, sr,
 ):
     at = Place(*sizes).here()
@@ -181,10 +181,12 @@
     experts = own_gate.shape[0]
     cap = rows // experts
     cuts = tiles_of(width)
+    pairs = (
+        (far_gate, gate_ref), (far_up, up_ref), (far_down, down_ref),
+        (wide_gate, own_gate), (wide_up, own_up), (wide_down, own_down),
+    )
     loads = [
-        pltpu.make_async_copy(wide_gate, own_gate, weight_sem.at[0]),
-        pltpu.make_async_copy(wide_up, own_up, weight_sem.at[1]),
-        pltpu.make_async_copy(wide_down, own_down, weight_sem.at[2]),
+        pltpu.make_async_copy(src, dst, weight_sem.at[i]) for i, (src, dst) in enumerate(pairs)
     ]
     for load in loads:
         load.start()
@@ -280,7 +282,7 @@
             came_ref.at[side, owner, :, cuts[i]],
             ss.at[owner, i],
             sr.at[side, owner, i],
-            at.column(at.a + (-1 if side == 0 else 1)),
+            at.column(at.a - 1 + 2 * side),
         )
 
     def step(owner, side, more):
@@ -293,8 +295,11 @@
             toward(owner, side, i).start()
 
     def homeward(turn):
-        for owner, side, far in ((last - turn, 0, has_right), (turn, 1, has_left)):
-            goes = (owner < at.a) if side == 0 else (owner > at.a)
+        for place in range(2):
+            side = jnp.where(2 * at.a < at.deep, 1 - place, place)
+            owner = jnp.where(side == 0, last - turn, turn)
+            goes = jnp.where(side == 0, owner < at.a, owner > at.a)
+            far = jnp.where(side == 0, has_right, has_left)
             pl.when(goes & far)(lambda owner=owner, side=side: step(owner, side, True))
             pl.when(goes & jnp.logical_not(far))(
                 lambda owner=owner, side=side: step(owner, side, False)
@@ -308,6 +313,8 @@
     order = [at.nearest(i) for i in range(at.deep)]
     forward(x_ref, at.a)
     pass_on(at.a, x_ref)
+    for load in loads[:3]:
+        load.wait()
     for cut in tiles_of(gate_ref.shape[1], 256):
         gate = jnp.dot(x_ref[...], gate_ref[:, cut], preferred_element_type=jnp.float32)
         up = jnp.dot(x_ref[...], up_ref[:, cut], preferred_element_type=jnp.float32)
@@ -320,7 +327,7 @@
         if i < at.deep:
             take(i)
         if i == 1:
-            for load in loads:
+            for load in loads[3:]:
                 load.wait()
         if i == at.deep:
             for turn in range(1, at.deep - 2):
@@ -371,7 +378,7 @@
     return pl.pallas_call(
         functools.partial(experts_kernel, sizes),
         out_shape=jax.ShapeDtypeStruct((tokens, width), half),
-        in_specs=[vmem] * 7 + [far] * 3,
+        in_specs=[vmem] * 4 + [far] * 6,
         out_specs=vmem,
         scratch_shapes=[
             pltpu.VMEM(chunk, half),
@@ -384,10 +391,13 @@
             pltpu.VMEM((tokens, width), jnp.float32),
             pltpu.VMEM((experts, slots // experts, routed[0].shape[2]), half),
             pltpu.VMEM((tokens, common[0].shape[1]), half),
+            pltpu.VMEM(common[0].shape, half),
+            pltpu.VMEM(common[1].shape, half),
+            pltpu.VMEM(common[2].shape, half),
             pltpu.VMEM(routed[0].shape, half),
             pltpu.VMEM(routed[1].shape, half),
             pltpu.VMEM(routed[2].shape, half),
-            dma((3,)),
+            dma((6,)),
             dma((2, at.deep)),
             dma((at.deep,)),
             dma((at.deep, at.flat)),

time: 169 us -> 158 us (0.935)
  Pallas kernels: 144 us -> 133 us
    pallas_call x1, Pallas kernels: 126 us -> 115 us  [experts_layer(): pl.pallas_call(functools.partial(experts_kernel, sizes), out_shape=jax.Sh...]
where the time goes in v2:
time: 158 us; the launch traced here: 155 us
  Pallas kernels  133 us (84%)
  local copies, waits for them, and re-layouts  9.33 us (6%)
  other arithmetic  6.62 us (4%)
  matrix products  5.71 us (4%)
    pallas_call x1, Pallas kernels, experts_layer(): pl.pallas_call(functools.partial(experts_kernel, sizes), out_shape=jax.Sh...  115 us
    pallas_call x2, Pallas kernels, remote_call(): pl.pallas_call(kernel, out_shape=out_shape, in_specs=[vmem] * len(operand...  18 us
    dot_general x1, matrix products, on_device(): jnp.dot(swap_tp(stacked), mixer_output_weight, preferred_element_type=jnp...  3.19 us

profile of v2, /device:TPU:18, one launch (start us, length us, event | category | flops | bytes accessed | tf_op | source)
XLA Modules:
  0.0 155.2 jit_solution(3184089425865878159)
XLA Ops:
  0.0 0.0 copy-start
  0.0 1.1 copy.60
  1.1 0.9 fusion.34
  1.9 0.1 reshape.149
  2.1 0.2 copy.61
  2.3 0.0 copy-start.8
  2.3 0.0 copy-start.9
  2.3 0.6 convolution_bitcast_fusion
  3.0 1.2 reshape.162
  4.2 0.0 copy-done.5
  4.2 0.3 reshape.161
  4.6 0.0 copy-done.3
  4.6 0.1 reshape.151
  4.7 0.4 fusion.2
  5.1 0.3 fusion.12
  5.3 0.0 copy-start.4
  5.4 0.1 copy.80
  5.6 0.3 fusion.28
  5.9 0.6 convert_element_type.65
  6.5 0.0 copy-done.8
  6.5 0.1 reshape_squeeze.3
  6.6 0.1 pad.3.clone
  6.7 0.0 copy-done.9
  6.7 0.7 maximum_maximum_fusion.y_ref
  7.3 11.3 %shard_map.172 = (bf16[8,128,128]{2,1,0:T(8,128)(2,1)}, f32[8,16,128]{2,1,0:T(8,128)}) custom-call(bf16[128,128]{1,0:T(8,128)(2,1)} %bitcast.95, f32[16,128]{1,0:T(8,128)} %maximum_maximum_fusion.y_ref), custom_call_target="tpu_custom_call" | custom-call | tf_op jit(solution)/shard_map/pallas_call | solution.py:50
  18.6 0.8 slice_reduce_fusion
  19.4 0.1 reshape.152
  19.5 0.1 broadcast_select_fusion
  19.6 0.1 select_reduce_fusion
  19.7 0.1 exp.49
  19.8 0.1 broadcast_select_fusion.1
  19.9 1.2 multiply_reduce_fusion.1
  21.0 0.1 copy.69
  21.1 0.1 copy.67
  21.2 0.1 copy.66
  21.4 0.0 copy-start.2
  21.4 0.4 fusion.3
  21.8 0.4 multiply_reduce_fusion
  22.2 0.1 copy.86
  22.4 0.6 mul.131
  23.0 0.0 copy-start.7
  23.0 0.4 copy.72
  23.4 0.0 copy-done
  23.4 0.0 copy-done.4
  23.4 0.0 copy-start.6
  23.4 0.9 fusion.24
  24.3 6.7 %shard_map.173 = bf16[128,1024]{1,0:T(8,128)(2,1)} custom-call(bf16[4,128,256]{2,1,0:T(8,128)(2,1)} %bitcast.89), custom_call_target="tpu_custom_call" | custom-call | tf_op jit(solution)/shard_map/pallas_call | solution.py:50
  31.0 0.0 copy-done.2
  31.0 3.2 %fusion.4 = (f32[128]{0:T(128)S(1)}, bf16[128,2048]{1,0:T(8,128)(2,1)S(1)}) fusion(bf16[128,1024]{1,0:T(8,128)(2,1)} %shard_map.173, bf16[1024,2048]{1,0:T(8,128)(2,1)} %param.26, bf16[128,2048]{1,0:T(8,128)(2,1)S(1)} %copy-done.2), kind=kOutput, calls=%fused_computation.11 | convolution fusion | flops 538443648 | bytes 5505536 | tf_op jit(solution)/shard_map/dot_general | solution.py:513
  34.2 0.0 copy-start.1
  34.2 0.0 copy-done.7
  34.2 1.0 fusion.6.x_ref
  35.2 0.0 copy-done.6
  35.3 0.1 fusion.47
  35.4 0.1 copy.76
  35.6 0.3 copy.75
  35.9 0.1 fusion.50
  36.1 0.2 copy.74
  36.3 0.1 eq.40
  36.4 0.9 fusion.31
  37.3 0.9 copy.77.select_ref
  38.2 0.0 copy-done.1
  38.2 115.1 %shard_map.174 = bf16[128,2048]{1,0:T(8,128)(2,1)} custom-call(bf16[128,2048]{1,0:T(8,128)(2,1)} %fusion.6.x_ref, bf16[128,2048]{1,0:T(8,128)(2,1)} %copy-done.1, bf16[4,256,128]{2,1,0:T(8,128)(2,1)} %copy.77.select_ref, bf16[4,128,256]{2,1,0:T(8,128)(2,1)} %get-tuple-element.11.mix_ref, bf16[2048,512]{1,0:T(8,128)(2,1)} %far_gate.1, ...), custom_call_target="tpu_custom_call" | custom-call | tf_op jit(solution)/shard_map/pallas_call | solution.py:378
  153.3 1.9 %copy.127 = bf16[128,2048]{1,0:T(8,128)(2,1)} copy(bf16[128,2048]{1,0:T(8,128)(2,1)} %shard_map.174) | data formatting | bytes 1048576
  (30 shorter events, 0.4 us)
Async XLA Ops:
  0.0 23.4 %copy-start = (f32[128]{0:T(128)S(1)}, f32[128]{0:T(128)}, u32[]{:S(2)}) copy-start(f32[128]{0:T(128)} %param.24) | copy-start | bytes 1540
  0.0 4.2 %copy-start.5 = (bf16[512,128]{1,0:T(8,128)(2,1)S(1)}, bf16[512,128]{1,0:T(8,128)(2,1)}, u32[]{:S(2)}) copy-start(bf16[512,128]{1,0:T(8,128)(2,1)} %param.18) | copy-start | bytes 393220
  0.0 4.6 %copy-start.3 = (bf16[512,256]{1,0:T(8,128)(2,1)S(1)}, bf16[512,256]{1,0:T(8,128)(2,1)}, u32[]{:S(2)}) copy-start(bf16[512,256]{1,0:T(8,128)(2,1)} %param.20) | copy-start | bytes 786436
  2.3 4.2 %copy-start.8 = (s32[128,4]{0,1:T(4,128)S(1)}, s32[128,4]{0,1:T(4,128)}, u32[]{:S(2)}) copy-start(s32[128,4]{0,1:T(4,128)} %param.28) | copy-start | bytes 6148
  2.3 4.3 %copy-start.9 = (f32[128,4]{0,1:T(4,128)S(1)}, f32[128,4]{0,1:T(4,128)}, u32[]{:S(2)}) copy-start(f32[128,4]{0,1:T(4,128)} %param.29) | copy-start | bytes 6148
  5.3 18.1 %copy-start.4 = (bf16[512,256]{1,0:T(8,128)(2,1)S(1)}, bf16[512,256]{1,0:T(8,128)(2,1)}, u32[]{:S(2)}) copy-start(bf16[512,256]{1,0:T(8,128)(2,1)} %param.23) | copy-start | bytes 786436
  21.4 9.6 %copy-start.2 = (bf16[128,2048]{1,0:T(8,128)(2,1)S(1)}, bf16[128,2048]{1,0:T(8,128)(2,1)}, u32[]{:S(2)}) copy-start(bf16[128,2048]{1,0:T(8,128)(2,1)} %param.25) | copy-start | bytes 1572868
  23.0 11.3 %copy-start.7 = (f32[2048]{0:T(1024)S(1)}, f32[2048]{0:T(1024)}, u32[]{:S(2)}) copy-start(f32[2048]{0:T(1024)} %param.27) | copy-start | bytes 24580
  23.4 11.8 %copy-start.6 = (f32[8,16,128]{2,1,0:T(8,128)S(1)}, f32[8,16,128]{2,1,0:T(8,128)}, u32[]{:S(2)}) copy-start(f32[8,16,128]{2,1,0:T(8,128)} %get-tuple-element.7) | copy-start | bytes 196612
  34.2 4.0 %copy-start.1 = (bf16[128,2048]{1,0:T(8,128)(2,1)}, bf16[128,2048]{1,0:T(8,128)(2,1)S(1)}, u32[]{:S(2)}) copy-start(bf16[128,2048]{1,0:T(8,128)(2,1)S(1)} %get-tuple-element.20.middle_ref) | copy-start | bytes 1572868

commit v3 on v2

v3 whole, which is shorter than its diff:
```python
import functools
import math

import jax
import jax.numpy as jnp
from jax import lax
from jax.experimental import pallas as pl
from jax.experimental.pallas import tpu as pltpu
from jax.sharding import PartitionSpec as P

D = 2048
KEY_CHANNELS = 64
VDIM = 128
BLOCK = 64
TOP_K = 4


eps_norm = 1e-06
decay_running = 16.0
routed_scale = 2.5


def peer(sp, tp):
    return {"sp": sp, "tp": tp}


def call_on(targets):
    barrier = pltpu.get_barrier_semaphore()
    for target in targets:
        pl.semaphore_signal(
            barrier, inc=1, device_id=target, device_id_type=pl.DeviceIdType.MESH
        )
    return lambda: pl.semaphore_wait(barrier, len(targets))


def remote(src, dst, send, recv, target):
    return pltpu.make_async_remote_copy(
        src_ref=src,
        dst_ref=dst,
        send_sem=send,
        recv_sem=recv,
        device_id=target,
        device_id_type=pl.DeviceIdType.MESH,
    )


def dot_nt(a, b):
    return lax.dot_general(a, b, (((1,), (1,)), ((), ())), preferred_element_type=jnp.float32)


def dot_tn(a, b):
    return lax.dot_general(a, b, (((0,), (0,)), ((), ())), preferred_element_type=jnp.float32)


def exact_dot(ones, values):
    total = jnp.zeros((ones.shape[0], values.shape[1]), jnp.float32)
    for _ in range(3):
        part = values.astype(jnp.bfloat16)
        values = values - part.astype(jnp.float32)
        total = total + jnp.dot(ones, part, preferred_element_type=jnp.float32)
    return total


class Place:
    def __init__(self, sp_size, tp_size):
        self.deep = math.gcd(sp_size, 4)
        self.rows = sp_size // self.deep
        self.tp_size = tp_size
        self.flat = self.rows * tp_size

    def here(self):
        sp, tp = lax.axis_index("sp"), lax.axis_index("tp")
        self.sp, self.tp = sp, tp
        self.a = sp // self.rows
        self.b = lax.rem(sp, self.rows)
        self.p = self.b * self.tp_size + tp
        return self

    def column(self, a):
        return peer(a * self.rows + self.b, self.tp)

    def plane(self, p):
        return peer(self.a * self.rows + p // self.tp_size, lax.rem(p, self.tp_size))

    def across(self, q):
        return lax.rem(self.p + q, self.flat)

    def nearest(self, i):
        last = self.deep - 1
        span = jnp.minimum(self.a, last - self.a)
        zigzag = self.a + ((i + 1) // 2 if i % 2 else -(i // 2))
        return jnp.where(i <= 2 * span, zigzag, jnp.where(self.a < last - self.a, i, last - i))


def tiles_of(width, most=512):
    step = math.gcd(width, most)
    return [slice(i, i + step) for i in range(0, width, step)]


def flatten_rows(block):
    groups, rows, width = block.shape
    if rows % 16 == 0:
        return block.reshape(groups * rows, width)
    return block.astype(jnp.float32).reshape(groups * rows, width).astype(jnp.bfloat16)


def layer_kernel(
    sizes, q_ref, k_ref, v_ref, decay_ref, offset_ref, open_ref, head_gain_ref, residual_ref,
    gain_ref, packet_ref, far_mix, far_gate, far_up, far_down,
    wide_gate, wide_up, wide_down, out_ref,
    qd_ref, qx_ref, kg_ref, kt_ref, ends_ref, starts_ref, inner_ref, state_ref, log_ref,
    states_ref, logs_ref, carried_ref, reach_ref, packets_ref, gated_ref, swapped_ref,
    mixer_ref, x_ref, middle_ref, select_ref, mix_ref,
    column_ref, stage_ref, arrived_ref, made_ref, back_ref, sent_ref, came_ref, base_ref,
    hidden_ref, shared_ref, gate_ref, up_ref, down_ref, own_gate, own_up, own_down,
    weight_sem, ks, kr, gs, gr, ls, lr, ws, wr, zs, zr, ps, pr, bs, br, ss, sr,
):
    at = Place(*sizes).here()
    last = at.deep - 1
    flat, rows = stage_ref.shape[1], stage_ref.shape[2]
    width = x_ref.shape[1]
    experts = own_gate.shape[0]
    cap = rows // experts
    cuts = tiles_of(width)
    pairs = (
        (far_mix, mixer_ref), (far_gate, gate_ref), (far_up, up_ref), (far_down, down_ref),
        (wide_gate, own_gate), (wide_up, own_up), (wide_down, own_down),
    )
    loads = [
        pltpu.make_async_copy(src, dst, weight_sem.at[i]) for i, (src, dst) in enumerate(pairs)
    ]
    for load in loads:
        load.start()
    has_right, has_left = at.a < last, at.a > 0
    count, tps = sizes
    met = call_on(
        [peer(lax.rem(at.sp + d, count), at.tp) for d in range(1, count)]
        + [at.plane(at.across(q)) for q in range(1, flat)]
    )
    half, wide = jnp.bfloat16, jnp.float32
    length, lanes = q_ref.shape
    heads = offset_ref.shape[1]
    blocks = length // BLOCK
    tokens = x_ref.shape[0]
    lane = lax.broadcasted_iota(jnp.int32, (1, lanes), 1)
    of_head = [
        (lane >= h * KEY_CHANNELS) & (lane < (h + 1) * KEY_CHANNELS) for h in range(heads)
    ]
    columns = [slice(h * VDIM, (h + 1) * VDIM) for h in range(heads)]
    tile = math.gcd(length, 4 * BLOCK)
    row = lax.broadcasted_iota(jnp.int32, (tile, tile), 0)
    col = lax.broadcasted_iota(jnp.int32, (tile, tile), 1)
    causal = (jnp.bitwise_and(row, -BLOCK) == jnp.bitwise_and(col, -BLOCK)) & (col <= row)
    ones = jnp.where(causal, 1.0, 0.0).astype(half)

    for t in range(0, length, tile):
        span = slice(t, t + tile)
        pre = decay_ref[span, :].astype(wide)
        offset = jnp.zeros((tile, lanes), wide)
        for h in range(heads):
            offset = jnp.where(of_head[h], offset_ref[span, h : h + 1], offset)
        log_decay = (
            jnp.minimum(pre, 0.0) - jnp.log1p(jnp.exp(-jnp.abs(pre)))
        ) / decay_running + offset
        within = exact_dot(ones, log_decay)
        keys = k_ref[span, :].astype(wide)
        qd_ref[span, :] = q_ref[span, :].astype(wide) * KEY_CHANNELS ** (-0.5) * jnp.exp(within)
        grown = keys * jnp.exp(-within)
        for h in range(heads):
            kg_ref[h, span, :] = jnp.where(of_head[h], grown, 0.0).astype(half)
        for n in range(0, tile, BLOCK):
            inside = slice(n, n + BLOCK)
            end = within[n + BLOCK - 1 : n + BLOCK, :]
            kt_ref[t + n : t + n + BLOCK, :] = (
                keys[inside, :] * jnp.exp(end - within[inside, :])
            ).astype(half)
            ends_ref[(t + n) // BLOCK : (t + n) // BLOCK + 1, :] = end
    state = jnp.zeros((VDIM, lanes), wide)
    passed = jnp.zeros((1, lanes), wide)
    for n in range(blocks):
        span = slice(n * BLOCK, (n + 1) * BLOCK)
        starts_ref[n] = state.astype(half)
        end = ends_ref[n : n + 1, :]
        both = dot_tn(v_ref[span, :], kt_ref[span, :])
        added = both[columns[0], :]
        for h in range(1, heads):
            added = jnp.where(of_head[h], both[columns[h], :], added)
        moved = qd_ref[span, :] * jnp.exp(passed)
        for h in range(heads):
            qx_ref[h, span, :] = jnp.where(of_head[h], moved, 0.0).astype(half)
        state = state * jnp.exp(end) + added
        passed = passed + end
    state_ref[...] = state.astype(half)
    log_ref[...] = jnp.broadcast_to(passed, log_ref.shape)
    met()

    def packet_copy(d):
        return remote(
            packet_ref,
            packets_ref.at[at.a],
            ks.at[d],
            kr.at[at.a],
            at.column(lax.rem(at.a + d, at.deep)),
        )

    def packet_from(a):
        return remote(packet_ref, packets_ref.at[a], ks.at[0], kr.at[a], at.column(at.a))

    def state_copy(d):
        target = peer(jnp.minimum(at.sp + d, count - 1), at.tp)
        return (
            remote(state_ref, states_ref.at[at.sp], gs.at[d], gr.at[at.sp], target),
            remote(log_ref, logs_ref.at[at.sp], ls.at[d], lr.at[at.sp], target),
        )

    def swap_copy(d):
        to = lax.rem(at.tp + d, tps)
        return remote(
            gated_ref.at[to], swapped_ref.at[at.tp], ws.at[d], wr.at[at.tp], peer(at.sp, to)
        )

    for d in range(1, at.deep):
        packet_copy(d).start()
    for d in range(1, count):

        @pl.when(at.sp + d < count)
        def _(d=d):
            for copy in state_copy(d):
                copy.start()

    packets_ref[at.a] = packet_ref[...]
    for t in range(0, length, tile):
        span = slice(t, t + tile)
        ahead = qd_ref[span, :].astype(half)
        for h in range(heads):
            scores = jnp.where(causal, dot_nt(ahead, kg_ref[h, span, :]), 0.0)
            inner_ref[span, columns[h]] = jnp.dot(
                scores.astype(half), v_ref[span, columns[h]], preferred_element_type=wide
            )
    for n in range(1, blocks):
        span = slice(n * BLOCK, (n + 1) * BLOCK)
        for h in range(heads):
            ahead = jnp.where(of_head[h], qd_ref[span, :], 0.0).astype(half)
            inner_ref[span, columns[h]] += dot_nt(ahead, starts_ref[n])

    slots = flat * rows
    plane_experts = flat * experts
    here = lax.broadcasted_iota(jnp.int32, (slots, plane_experts), 0)
    there = lax.broadcasted_iota(jnp.int32, (slots, plane_experts), 1) * cap
    belongs = (here >= there) & (here < there + cap)
    spread = jnp.where(belongs, 1.0, 0.0).astype(half)
    place = jnp.sum(
        jnp.where(belongs, (here - there).astype(wide), 0.0), axis=1, keepdims=True
    )
    expert = (
        at.a * plane_experts + lax.broadcasted_iota(jnp.int32, (plane_experts, 1), 0)
    ).astype(wide)
    sooner = jnp.where(
        lax.broadcasted_iota(jnp.int32, (tokens, tokens), 0)
        < lax.broadcasted_iota(jnp.int32, (tokens, tokens), 1),
        1.0,
        0.0,
    ).astype(half)
    for a in range(at.deep):
        pl.when(at.a != a)(lambda a=a: packet_from(a).wait_recv())
        scored = packets_ref[a, TOP_K:, :]
        share = routed_scale * scored / jnp.sum(scored, axis=0, keepdims=True)
        chosen = jnp.zeros((plane_experts, tokens), wide)
        weight_of = jnp.zeros((plane_experts, tokens), wide)
        for k in range(TOP_K):
            hit = packets_ref[a, k : k + 1, :] == expert
            chosen = jnp.where(hit, 1.0, chosen)
            weight_of = jnp.where(hit, share[k : k + 1, :], weight_of)
        rank = jnp.dot(chosen.astype(half), sooner, preferred_element_type=wide)
        rank = jnp.where(chosen > 0.0, rank, -1.0)
        ranks = jnp.dot(spread, rank.astype(half), preferred_element_type=wide)
        weights = jnp.dot(spread, weight_of.astype(half), preferred_element_type=wide)
        taken = ranks == place
        select_ref[a] = jnp.where(taken, 1.0, 0.0).astype(half)
        mix_ref[a] = jnp.transpose(jnp.where(taken, weights, 0.0)).astype(half)

    carried_ref[...] = jnp.zeros_like(carried_ref)
    reach_ref[...] = jnp.zeros_like(reach_ref)
    for j in reversed(range(count - 1)):

        @pl.when(j < at.sp)
        def _(j=j):
            source = peer(j, at.tp)
            remote(state_ref, states_ref.at[j], gs.at[0], gr.at[j], source).wait_recv()
            remote(log_ref, logs_ref.at[j], ls.at[0], lr.at[j], source).wait_recv()
            carried_ref[...] += jnp.exp(reach_ref[0:1, :]) * states_ref[j].astype(wide)
            reach_ref[...] += logs_ref[j]

    carried = carried_ref[...].astype(half)
    for d in [*range(1, tps), 0]:
        to = lax.rem(at.tp + d, tps)
        span = pl.ds(pl.multiple_of(to * tokens, tokens), tokens)
        for h in range(heads):
            output = inner_ref[span, columns[h]] + dot_nt(qx_ref[h, span, :], carried)
            inv_rms = lax.rsqrt(jnp.mean(output * output, axis=-1, keepdims=True) + eps_norm)
            gated_ref[to, :, columns[h]] = (
                output
                * inv_rms
                * head_gain_ref[...]
                * jax.nn.silu(open_ref[span, columns[h]].astype(wide))
            ).astype(half)
        if d > 0:
            swap_copy(d).start()
    loads[0].wait()
    span = heads * VDIM
    for d in range(tps):
        source = lax.rem(at.tp - d + tps, tps)
        if d > 0:
            remote(
                gated_ref.at[0], swapped_ref.at[source], ws.at[0], wr.at[source], peer(at.sp, source)
            ).wait_recv()
        piece = gated_ref[source] if d == 0 else swapped_ref[source]
        part_of = pl.ds(pl.multiple_of(source * span, span), span)
        for cut in cuts:
            part = jnp.dot(piece, mixer_ref[part_of, cut], preferred_element_type=wide)
            if d == 0:
                base_ref[:, cut] = residual_ref[:, cut].astype(wide) + part
            else:
                base_ref[:, cut] += part
    square = jnp.zeros((tokens, 1), wide)
    for cut in cuts:
        middle_ref[:, cut] = base_ref[:, cut].astype(half)
        middle = middle_ref[:, cut].astype(wide)
        square = square + jnp.sum(middle * middle, axis=-1, keepdims=True)
    scale = lax.rsqrt(square / width + eps_norm)
    for cut in cuts:
        x_ref[:, cut] = (middle_ref[:, cut].astype(wide) * scale * gain_ref[:, cut]).astype(half)

    def relay(source, owner, side):
        return remote(
            source,
            column_ref.at[owner],
            zs.at[side, owner],
            zr.at[owner],
            at.column(at.a + (1 if side == 0 else -1)),
        )

    def sends(owner):
        right = has_right & (owner <= at.a)
        left = has_left & (owner >= at.a)
        return right, left

    def forward(source, owner):
        right, left = sends(owner)
        pl.when(right)(lambda: relay(source, owner, 0).start())
        pl.when(left)(lambda: relay(source, owner, 1).start())

    def out_copy(owner, q):
        target = at.across(q)
        return remote(
            stage_ref.at[owner, target],
            arrived_ref.at[owner, at.p],
            ps.at[owner, q],
            pr.at[owner, q],
            at.plane(target),
        )

    def back_copy(owner, q, i):
        target = at.across(q)
        return remote(
            made_ref.at[owner, target, :, cuts[i]],
            back_ref.at[owner, at.p, :, cuts[i]],
            bs.at[owner, q, i],
            br.at[owner, q, i],
            at.plane(target),
        )

    def pass_on(owner, source):
        for cut in cuts:
            picked = jnp.dot(
                select_ref[owner], source[:, cut], preferred_element_type=jnp.float32
            )
            stage_ref[owner, :, :, cut] = picked.reshape(flat, rows, -1).astype(jnp.bfloat16)
        for q in range(1, flat):
            out_copy(owner, q).start()
        arrived_ref[owner, at.p] = stage_ref[owner, at.p]

    def send_back(owner, i):
        for q in range(1, flat):
            back_copy(owner, q, i).start()

    def run_experts(owner, hold=False):
        for q in range(1, flat):
            out_copy(owner, q).wait_recv()
        for e in range(experts):
            mine = slice(e * cap, (e + 1) * cap)
            block = flatten_rows(arrived_ref[owner, :, mine, :])
            for cut in tiles_of(own_gate.shape[2], 256):
                gate = jnp.dot(block, own_gate[e, :, cut], preferred_element_type=jnp.float32)
                up = jnp.dot(block, own_up[e, :, cut], preferred_element_type=jnp.float32)
                hidden_ref[e, :, cut] = (jax.nn.silu(gate) * up).astype(jnp.bfloat16)
        for i, cut in enumerate(cuts):
            for e in range(experts):
                mine = slice(e * cap, (e + 1) * cap)
                down = jnp.dot(
                    hidden_ref[e], own_down[e, :, cut], preferred_element_type=jnp.float32
                )
                made_ref[owner, :, mine, cut] = down.reshape(flat, cap, -1).astype(jnp.bfloat16)
            if not hold:
                send_back(owner, i)
        back_ref[owner, at.p] = made_ref[owner, at.p]

    def mixed(owner, i):
        for q in range(1, flat):
            back_copy(owner, q, i).wait_recv()
        block = flatten_rows(back_ref[owner, :, :, cuts[i]])
        return jnp.dot(mix_ref[owner], block, preferred_element_type=jnp.float32)

    def toward(owner, side, i):
        return remote(
            sent_ref.at[owner, :, cuts[i]],
            came_ref.at[side, owner, :, cuts[i]],
            ss.at[owner, i],
            sr.at[side, owner, i],
            at.column(at.a - 1 + 2 * side),
        )

    def step(owner, side, more):
        for i, cut in enumerate(cuts):
            part = mixed(owner, i)
            if more:
                toward(owner, side, i).wait_recv()
                part = part + came_ref[side, owner, :, cut].astype(jnp.float32)
            sent_ref[owner, :, cut] = part.astype(jnp.bfloat16)
            toward(owner, side, i).start()

    def homeward(turn):
        for place in range(2):
            side = jnp.where(2 * at.a < at.deep, 1 - place, place)
            owner = jnp.where(side == 0, last - turn, turn)
            goes = jnp.where(side == 0, owner < at.a, owner > at.a)
            far = jnp.where(side == 0, has_right, has_left)
            pl.when(goes & far)(lambda owner=owner, side=side: step(owner, side, True))
            pl.when(goes & jnp.logical_not(far))(
                lambda owner=owner, side=side: step(owner, side, False)
            )

    def take(i):
        relay(x_ref, order[i], 0).wait_recv()
        forward(column_ref.at[order[i]], order[i])
        pass_on(order[i], column_ref.at[order[i]])

    order = [at.nearest(i) for i in range(at.deep)]
    forward(x_ref, at.a)
    pass_on(at.a, x_ref)
    for load in loads[1:4]:
        load.wait()
    for cut in tiles_of(gate_ref.shape[1], 256):
        gate = jnp.dot(x_ref[...], gate_ref[:, cut], preferred_element_type=jnp.float32)
        up = jnp.dot(x_ref[...], up_ref[:, cut], preferred_element_type=jnp.float32)
        shared_ref[:, cut] = (jax.nn.silu(gate) * up).astype(jnp.bfloat16)
    for cut in cuts:
        base_ref[:, cut] = middle_ref[:, cut].astype(jnp.float32) + jnp.dot(
            shared_ref[...], down_ref[:, cut], preferred_element_type=jnp.float32
        )
    for i in range(1, at.deep + 1):
        if i < at.deep:
            take(i)
        if i == 1:
            for load in loads[4:]:
                load.wait()
        if i == at.deep:
            for turn in range(1, at.deep - 2):
                homeward(turn)
        run_experts(order[i - 1], hold=i == 1)
    for i in range(len(cuts)):
        send_back(at.a, i)
    for turn in range(max(1, at.deep - 2), at.deep):
        homeward(turn)

    for side, far in ((0, has_right), (1, has_left)):

        @pl.when(far)
        def _(side=side):
            for i, cut in enumerate(cuts):
                toward(at.a, side, i).wait_recv()
                base_ref[:, cut] += came_ref[side, at.a, :, cut].astype(jnp.float32)

    for i, cut in enumerate(cuts):
        out_ref[:, cut] = (base_ref[:, cut] + mixed(at.a, i)).astype(out_ref.dtype)
    for d in range(1, at.deep):
        packet_copy(d).wait_send()
    for d in range(1, count):

        @pl.when(at.sp + d < count)
        def _(d=d):
            for copy in state_copy(d):
                copy.wait_send()

    for d in range(1, tps):
        swap_copy(d).wait_send()
    for i in range(at.deep):
        owner = order[i]
        right, left = sends(owner)
        pl.when(right)(lambda owner=owner: relay(x_ref, owner, 0).wait_send())
        pl.when(left)(lambda owner=owner: relay(x_ref, owner, 1).wait_send())
        for q in range(1, flat):
            out_copy(owner, q).wait_send()
            for j in range(len(cuts)):
                back_copy(owner, q, j).wait_send()
        if i > 0:
            for j in range(len(cuts)):
                toward(owner, 0, j).wait_send()


def on_device(
    queries,
    key_matrix,
    value_matrix,
    channel_decay_input,
    head_decay_offset,
    output_gate_input,
    head_norm_gain,
    residual,
    mixer_output_weight,
    expert_norm_gain,
    routes,
    chosen_router_scores,
    routed_gate_weight,
    routed_up_weight,
    routed_down_weight,
    common_gate_weight,
    common_up_weight,
    common_down_weight,
):
    count, tps = sizes = (lax.axis_size("sp"), lax.axis_size("tp"))
    at = Place(*sizes)
    tokens, width = residual.shape
    length, lanes = queries.shape
    heads = head_decay_offset.shape[1]
    blocks = length // BLOCK
    experts = routed_gate_weight.shape[0]
    cap = 2 * TOP_K * tokens // (experts * count * tps)
    rows = experts * cap
    slots = at.flat * rows
    parts = len(tiles_of(width))
    packet = jnp.concatenate(
        [routes.T.astype(jnp.float32), chosen_router_scores.T], axis=0
    )
    common = (common_gate_weight, common_up_weight, common_down_weight)
    routed = (routed_gate_weight, routed_up_weight, routed_down_weight)
    box = (at.deep, at.flat, rows, width)
    chunk = (at.deep, tokens, width)
    dma = pltpu.SemaphoreType.DMA
    half, wide = jnp.bfloat16, jnp.float32
    vmem = pl.BlockSpec(memory_space=pltpu.VMEM)
    far = pl.BlockSpec(memory_space=pl.ANY)
    return pl.pallas_call(
        functools.partial(layer_kernel, sizes),
        out_shape=jax.ShapeDtypeStruct((tokens, width), half),
        in_specs=[vmem] * 10 + [far] * 7,
        out_specs=vmem,
        scratch_shapes=[
            pltpu.VMEM((length, lanes), wide),
            pltpu.VMEM((heads, length, lanes), half),
            pltpu.VMEM((heads, length, lanes), half),
            pltpu.VMEM((length, lanes), half),
            pltpu.VMEM((max(8, blocks), lanes), wide),
            pltpu.VMEM((blocks, VDIM, lanes), half),
            pltpu.VMEM((length, heads * VDIM), wide),
            pltpu.VMEM((VDIM, lanes), half),
            pltpu.VMEM((8, lanes), wide),
            pltpu.VMEM((count, VDIM, lanes), half),
            pltpu.VMEM((count, 8, lanes), wide),
            pltpu.VMEM((VDIM, lanes), wide),
            pltpu.VMEM((8, lanes), wide),
            pltpu.VMEM((at.deep,) + packet.shape, wide),
            pltpu.VMEM((tps, tokens, heads * VDIM), half),
            pltpu.VMEM((tps, tokens, heads * VDIM), half),
            pltpu.VMEM(mixer_output_weight.shape, half),
            pltpu.VMEM((tokens, width), half),
            pltpu.VMEM((tokens, width), half),
            pltpu.VMEM((at.deep, slots, tokens), half),
            pltpu.VMEM((at.deep, tokens, slots), half),
            pltpu.VMEM(chunk, half),
            pltpu.VMEM(box, half),
            pltpu.VMEM(box, half),
            pltpu.VMEM(box, half),
            pltpu.VMEM(box, half),
            pltpu.VMEM(chunk, half),
            pltpu.VMEM((2,) + chunk, half),
            pltpu.VMEM((tokens, width), wide),
            pltpu.VMEM((experts, at.flat * cap, routed[0].shape[2]), half),
            pltpu.VMEM((tokens, common[0].shape[1]), half),
            pltpu.VMEM(common[0].shape, half),
            pltpu.VMEM(common[1].shape, half),
            pltpu.VMEM(common[2].shape, half),
            pltpu.VMEM(routed[0].shape, half),
            pltpu.VMEM(routed[1].shape, half),
            pltpu.VMEM(routed[2].shape, half),
            dma((7,)),
            dma((at.deep,)),
            dma((at.deep,)),
            dma((count,)),
            dma((count,)),
            dma((count,)),
            dma((count,)),
            dma((tps,)),
            dma((tps,)),
            dma((2, at.deep)),
            dma((at.deep,)),
            dma((at.deep, at.flat)),
            dma((at.deep, at.flat)),
            dma((at.deep, at.flat, parts)),
            dma((at.deep, at.flat, parts)),
            dma((at.deep, parts)),
            dma((2, at.deep, parts)),
        ],
        compiler_params=pltpu.CompilerParams(
            collective_id=0, has_side_effects=True, vmem_limit_bytes=62 * 1024 * 1024
        ),
    )(
        queries,
        key_matrix,
        value_matrix,
        channel_decay_input,
        head_decay_offset,
        output_gate_input,
        head_norm_gain.reshape(1, -1),
        residual,
        expert_norm_gain.reshape(1, -1),
        packet,
        mixer_output_weight,
        *common,
        *routed,
    )


def solution(mesh):
    placed = (
        P("sp", "tp"),
        P("sp", "tp"),
        P("sp", "tp"),
        P("sp", "tp"),
        P("sp", "tp"),
        P("sp", "tp"),
        P(),
        P(("sp", "tp"), None),
        P(),
        P(),
        P(("sp", "tp"), None),
        P(("sp", "tp"), None),
        P(("sp", "tp"), None, None),
        P(("sp", "tp"), None, None),
        P(("sp", "tp"), None, None),
        P(),
        P(),
        P(),
    )
    return jax.shard_map(
        on_device, mesh=mesh, in_specs=placed, out_specs=P(("sp", "tp"), None), check_vma=False
    )
```

time: 158 us -> 136 us (0.86)
  local copies, waits for them, and re-layouts: 9.33 us -> 3.42 us
  matrix products: 5.71 us -> 0 us
  Pallas kernels: 133 us -> 128 us
  other arithmetic: 6.62 us -> 1.96 us
    dot_general x8 -> x0, matrix products: 5.71 us -> none  [the longest x1 3.19 us: on_device(): jnp.dot(swap_tp(stacked), mixer_output_weight, preferred_element_type=jnp...]
    pallas_call x3 -> x1, Pallas kernels: 133 us -> 128 us  [on_device(): pl.pallas_call(functools.partial(layer_kernel, sizes), out_shape=jax.Shap...]
    convert_element_type x6 -> x1, other arithmetic: 2.54 us -> 0.68 us  [on_device(): routes.T.astype(jnp.float32)]
    unnamed x22 -> x2, local copies, waits for them, and re-layouts: 2.99 us -> 3.42 us
where the time goes in v3:
time: 136 us; the launch traced here: 134 us
  Pallas kernels  128 us (94%)
  local copies, waits for them, and re-layouts  3.42 us (3%)
  other arithmetic  1.96 us (1%)
    pallas_call x1, Pallas kernels, on_device(): pl.pallas_call(functools.partial(layer_kernel, sizes), out_shape=jax.Shap...  128 us
    unnamed x2, local copies, waits for them, and re-layouts  3.42 us

profile of v3, /device:TPU:18, one launch (start us, length us, event | category | flops | bytes accessed | tf_op | source)
XLA Modules:
  0.0 133.7 jit_solution(1223672255286105757)
XLA Ops:
  0.0 0.7 convert_bitcast_fusion
  0.7 1.3 pad_maximum_fusion.packet_ref
  2.0 1.5 %copy.19.offset_ref = f32[512,2]{1,0:T(8,128)} copy(f32[512,2]{0,1:T(2,128)} %param.22) | data formatting | bytes 8192 | tf_op args[4]
  3.5 128.3 %shard_map.172 = bf16[128,2048]{1,0:T(8,128)(2,1)} custom-call(bf16[512,128]{1,0:T(8,128)(2,1)} %q_ref.1, bf16[512,128]{1,0:T(8,128)(2,1)} %k_ref.1, bf16[512,256]{1,0:T(8,128)(2,1)} %v_ref.1, bf16[512,128]{1,0:T(8,128)(2,1)} %decay_ref.1, f32[512,2]{1,0:T(8,128)} %copy.19.offset_ref, bf16[512,256]{1,0:T(8,128)(2,1)} %open_ref.1, f32[1,128]{1,0:T(1,128)} %bitcast.7, ...), custom_call_target="tpu_custom_call" | custom-call | tf_op jit(solution)/shard_map/pallas_call | solution.py:553
  131.8 1.9 %copy.21 = bf16[128,2048]{1,0:T(8,128)(2,1)} copy(bf16[128,2048]{1,0:T(8,128)(2,1)} %shard_map.172) | data formatting | bytes 1048576

commit v4 on v3

--- a/solution.py
+++ b/solution.py
@@ -52,12 +52,16 @@
     return lax.dot_general(a, b, (((0,), (0,)), ((), ())), preferred_element_type=jnp.float32)
 
 
-def exact_dot(ones, values):
-    total = jnp.zeros((ones.shape[0], values.shape[1]), jnp.float32)
+def dot_nn(a, b):
+    return jnp.dot(a, b, preferred_element_type=jnp.float32)
+
+
+def exact_dot(ones, values, dot):
+    total = 0.0
     for _ in range(3):
         part = values.astype(jnp.bfloat16)
         values = values - part.astype(jnp.float32)
-        total = total + jnp.dot(ones, part, preferred_element_type=jnp.float32)
+        total = total + dot(ones, part)
     return total
 
 
@@ -87,9 +91,11 @@
 
     def nearest(self, i):
         last = self.deep - 1
-        span = jnp.minimum(self.a, last - self.a)
-        zigzag = self.a + ((i + 1) // 2 if i % 2 else -(i // 2))
-        return jnp.where(i <= 2 * span, zigzag, jnp.where(self.a < last - self.a, i, last - i))
+        low = self.a < last - self.a
+        span = jnp.where(low, self.a, last - self.a)
+        away = (i + 1) // 2 if i % 2 else -(i // 2)
+        zigzag = jnp.where(low, self.a - away, self.a + away)
+        return jnp.where(i <= 2 * span, zigzag, jnp.where(low, i, last - i))
 
 
 def tiles_of(width, most=512):
@@ -106,10 +112,10 @@
 
 def layer_kernel(
     sizes, q_ref, k_ref, v_ref, decay_ref, offset_ref, open_ref, head_gain_ref, residual_ref,
-    gain_ref, packet_ref, far_mix, far_gate, far_up, far_down,
+    gain_ref, routes_ref, scores_ref, far_mix, far_gate, far_up, far_down,
     wide_gate, wide_up, wide_down, out_ref,
     qd_ref, qx_ref, kg_ref, kt_ref, ends_ref, starts_ref, inner_ref, state_ref, log_ref,
-    states_ref, logs_ref, carried_ref, reach_ref, packets_ref, gated_ref, swapped_ref,
+    states_ref, logs_ref, carried_ref, reach_ref, packet_ref, packets_ref, gated_ref, swapped_ref,
     mixer_ref, x_ref, middle_ref, select_ref, mix_ref,
     column_ref, stage_ref, arrived_ref, made_ref, back_ref, sent_ref, came_ref, base_ref,
     hidden_ref, shared_ref, gate_ref, up_ref, down_ref, own_gate, own_up, own_down,
@@ -122,6 +128,7 @@
     experts = own_gate.shape[0]
     cap = rows // experts
     cuts = tiles_of(width)
+    sides = tiles_of(width, 1024)
     pairs = (
         (far_mix, mixer_ref), (far_gate, gate_ref), (far_up, up_ref), (far_down, down_ref),
         (wide_gate, own_gate), (wide_up, own_up), (wide_down, own_down),
@@ -139,7 +146,7 @@
     )
     half, wide = jnp.bfloat16, jnp.float32
     length, lanes = q_ref.shape
-    heads = offset_ref.shape[1]
+    heads = offset_ref.shape[0]
     blocks = length // BLOCK
     tokens = x_ref.shape[0]
     lane = lax.broadcasted_iota(jnp.int32, (1, lanes), 1)
@@ -156,13 +163,14 @@
     for t in range(0, length, tile):
         span = slice(t, t + tile)
         pre = decay_ref[span, :].astype(wide)
-        offset = jnp.zeros((tile, lanes), wide)
-        for h in range(heads):
-            offset = jnp.where(of_head[h], offset_ref[span, h : h + 1], offset)
         log_decay = (
             jnp.minimum(pre, 0.0) - jnp.log1p(jnp.exp(-jnp.abs(pre)))
-        ) / decay_running + offset
-        within = exact_dot(ones, log_decay)
+        ) / decay_running
+        dropped = exact_dot(ones, offset_ref[:, span], dot_nt)
+        offset = dropped[:, 0:1]
+        for h in range(1, heads):
+            offset = jnp.where(of_head[h], dropped[:, h : h + 1], offset)
+        within = exact_dot(ones, log_decay, dot_nn) + offset
         keys = k_ref[span, :].astype(wide)
         qd_ref[span, :] = q_ref[span, :].astype(wide) * KEY_CHANNELS ** (-0.5) * jnp.exp(within)
         grown = keys * jnp.exp(-within)
@@ -192,8 +200,6 @@
         passed = passed + end
     state_ref[...] = state.astype(half)
     log_ref[...] = jnp.broadcast_to(passed, log_ref.shape)
-    met()
-
     def packet_copy(d):
         return remote(
             packet_ref,
@@ -219,15 +225,8 @@
             gated_ref.at[to], swapped_ref.at[at.tp], ws.at[d], wr.at[at.tp], peer(at.sp, to)
         )
 
-    for d in range(1, at.deep):
-        packet_copy(d).start()
-    for d in range(1, count):
-
-        @pl.when(at.sp + d < count)
-        def _(d=d):
-            for copy in state_copy(d):
-                copy.start()
-
+    packet_ref[:TOP_K, :] = routes_ref[...].astype(wide)
+    packet_ref[TOP_K:, :] = scores_ref[...]
     packets_ref[at.a] = packet_ref[...]
     for t in range(0, length, tile):
         span = slice(t, t + tile)
@@ -242,6 +241,16 @@
         for h in range(heads):
             ahead = jnp.where(of_head[h], qd_ref[span, :], 0.0).astype(half)
             inner_ref[span, columns[h]] += dot_nt(ahead, starts_ref[n])
+
+    met()
+    for d in range(1, at.deep):
+        packet_copy(d).start()
+    for d in range(1, count):
+
+        @pl.when(at.sp + d < count)
+        def _(d=d):
+            for copy in state_copy(d):
+                copy.start()
 
     slots = flat * rows
     plane_experts = flat * experts
@@ -261,7 +270,7 @@
         1.0,
         0.0,
     ).astype(half)
-    for a in range(at.deep):
+    def lay_out(a):
         pl.when(at.a != a)(lambda a=a: packet_from(a).wait_recv())
         scored = packets_ref[a, TOP_K:, :]
         share = routed_scale * scored / jnp.sum(scored, axis=0, keepdims=True)
@@ -279,6 +288,10 @@
         select_ref[a] = jnp.where(taken, 1.0, 0.0).astype(half)
         mix_ref[a] = jnp.transpose(jnp.where(taken, weights, 0.0)).astype(half)
 
+    early = at.deep // 2
+    for a in range(early):
+        lay_out(a)
+
     carried_ref[...] = jnp.zeros_like(carried_ref)
     reach_ref[...] = jnp.zeros_like(reach_ref)
     for j in reversed(range(count - 1)):
@@ -306,6 +319,8 @@
             ).astype(half)
         if d > 0:
             swap_copy(d).start()
+    for a in range(early, at.deep):
+        lay_out(a)
     loads[0].wait()
     span = heads * VDIM
     for d in range(tps):
@@ -331,12 +346,12 @@
     for cut in cuts:
         x_ref[:, cut] = (middle_ref[:, cut].astype(wide) * scale * gain_ref[:, cut]).astype(half)
 
-    def relay(source, owner, side):
+    def relay(source, owner, side, j):
         return remote(
-            source,
-            column_ref.at[owner],
-            zs.at[side, owner],
-            zr.at[owner],
+            source.at[:, sides[j]],
+            column_ref.at[owner, :, sides[j]],
+            zs.at[side, owner, j],
+            zr.at[owner, j],
             at.column(at.a + (1 if side == 0 else -1)),
         )
 
@@ -345,18 +360,18 @@
         left = has_left & (owner >= at.a)
         return right, left
 
-    def forward(source, owner):
+    def forward(source, owner, j):
         right, left = sends(owner)
-        pl.when(right)(lambda: relay(source, owner, 0).start())
-        pl.when(left)(lambda: relay(source, owner, 1).start())
-
-    def out_copy(owner, q):
+        pl.when(right)(lambda: relay(source, owner, 0, j).start())
+        pl.when(left)(lambda: relay(source, owner, 1, j).start())
+
+    def out_copy(owner, q, j):
         target = at.across(q)
         return remote(
-            stage_ref.at[owner, target],
-            arrived_ref.at[owner, at.p],
-            ps.at[owner, q],
-            pr.at[owner, q],
+            stage_ref.at[owner, target, :, sides[j]],
+            arrived_ref.at[owner, at.p, :, sides[j]],
+            ps.at[owner, q, j],
+            pr.at[owner, q, j],
             at.plane(target),
         )
 
@@ -370,23 +385,25 @@
             at.plane(target),
         )
 
-    def pass_on(owner, source):
-        for cut in cuts:
+    def pass_on(owner, source, j):
+        start, stop = sides[j].start, sides[j].stop
+        for cut in [cut for cut in cuts if start <= cut.start < stop]:
             picked = jnp.dot(
                 select_ref[owner], source[:, cut], preferred_element_type=jnp.float32
             )
             stage_ref[owner, :, :, cut] = picked.reshape(flat, rows, -1).astype(jnp.bfloat16)
         for q in range(1, flat):
-            out_copy(owner, q).start()
-        arrived_ref[owner, at.p] = stage_ref[owner, at.p]
+            out_copy(owner, q, j).start()
+        arrived_ref[owner, at.p, :, sides[j]] = stage_ref[owner, at.p, :, sides[j]]
 
     def send_back(owner, i):
         for q in range(1, flat):
             back_copy(owner, q, i).start()
 
-    def run_experts(owner, hold=False):
+    def run_experts(owner):
         for q in range(1, flat):
-            out_copy(owner, q).wait_recv()
+            for j in range(len(sides)):
+                out_copy(owner, q, j).wait_recv()
         for e in range(experts):
             mine = slice(e * cap, (e + 1) * cap)
             block = flatten_rows(arrived_ref[owner, :, mine, :])
@@ -401,9 +418,11 @@
                     hidden_ref[e], own_down[e, :, cut], preferred_element_type=jnp.float32
                 )
                 made_ref[owner, :, mine, cut] = down.reshape(flat, cap, -1).astype(jnp.bfloat16)
-            if not hold:
-                send_back(owner, i)
         back_ref[owner, at.p] = made_ref[owner, at.p]
+
+    def send_all(owner):
+        for i in range(len(cuts)):
+            send_back(owner, i)
 
     def mixed(owner, i):
         for q in range(1, flat):
@@ -441,13 +460,16 @@
             )
 
     def take(i):
-        relay(x_ref, order[i], 0).wait_recv()
-        forward(column_ref.at[order[i]], order[i])
-        pass_on(order[i], column_ref.at[order[i]])
+        for j in range(len(sides)):
+            relay(x_ref, order[i], 0, j).wait_recv()
+            forward(column_ref.at[order[i]], order[i], j)
+            pass_on(order[i], column_ref.at[order[i]], j)
 
     order = [at.nearest(i) for i in range(at.deep)]
-    forward(x_ref, at.a)
-    pass_on(at.a, x_ref)
+    for j in range(len(sides)):
+        forward(x_ref, at.a, j)
+    for j in range(len(sides)):
+        pass_on(at.a, x_ref, j)
     for load in loads[1:4]:
         load.wait()
     for cut in tiles_of(gate_ref.shape[1], 256):
@@ -465,12 +487,13 @@
             for load in loads[4:]:
                 load.wait()
         if i == at.deep:
-            for turn in range(1, at.deep - 2):
-                homeward(turn)
-        run_experts(order[i - 1], hold=i == 1)
-    for i in range(len(cuts)):
-        send_back(at.a, i)
-    for turn in range(max(1, at.deep - 2), at.deep):
+            send_all(order[1])
+        run_experts(order[i - 1])
+    turns = [1, *range(at.deep - 1, 1, -1)]
+    for turn in turns[1:]:
+        send_all(order[turn])
+    send_all(at.a)
+    for turn in turns:
         homeward(turn)
 
     for side, far in ((0, has_right), (1, has_left)):
@@ -497,10 +520,12 @@
     for i in range(at.deep):
         owner = order[i]
         right, left = sends(owner)
-        pl.when(right)(lambda owner=owner: relay(x_ref, owner, 0).wait_send())
-        pl.when(left)(lambda owner=owner: relay(x_ref, owner, 1).wait_send())
+        for j in range(len(sides)):
+            pl.when(right)(lambda owner=owner, j=j: relay(x_ref, owner, 0, j).wait_send())
+            pl.when(left)(lambda owner=owner, j=j: relay(x_ref, owner, 1, j).wait_send())
         for q in range(1, flat):
-            out_copy(owner, q).wait_send()
+            for j in range(len(sides)):
+                out_copy(owner, q, j).wait_send()
             for j in range(len(cuts)):
                 back_copy(owner, q, j).wait_send()
         if i > 0:
@@ -538,10 +563,7 @@
     cap = 2 * TOP_K * tokens // (experts * count * tps)
     rows = experts * cap
     slots = at.flat * rows
-    parts = len(tiles_of(width))
-    packet = jnp.concatenate(
-        [routes.T.astype(jnp.float32), chosen_router_scores.T], axis=0
-    )
+    parts, halves = len(tiles_of(width)), len(tiles_of(width, 1024))
     common = (common_gate_weight, common_up_weight, common_down_weight)
     routed = (routed_gate_weight, routed_up_weight, routed_down_weight)
     box = (at.deep, at.flat, rows, width)
@@ -552,8 +574,8 @@
     far = pl.BlockSpec(memory_space=pl.ANY)
     return pl.pallas_call(
         functools.partial(layer_kernel, sizes),
-        out_shape=jax.ShapeDtypeStruct((tokens, width), half),
-        in_specs=[vmem] * 10 + [far] * 7,
+        out_shape=pltpu.VMEM((tokens, width), half),
+        in_specs=[vmem] * 11 + [far] * 7,
         out_specs=vmem,
         scratch_shapes=[
             pltpu.VMEM((length, lanes), wide),
@@ -569,7 +591,8 @@
             pltpu.VMEM((count, 8, lanes), wide),
             pltpu.VMEM((VDIM, lanes), wide),
             pltpu.VMEM((8, lanes), wide),
-            pltpu.VMEM((at.deep,) + packet.shape, wide),
+            pltpu.VMEM((2 * TOP_K, tokens), wide),
+            pltpu.VMEM((at.deep, 2 * TOP_K, tokens), wide),
             pltpu.VMEM((tps, tokens, heads * VDIM), half),
             pltpu.VMEM((tps, tokens, heads * VDIM), half),
             pltpu.VMEM(mixer_output_weight.shape, half),
@@ -602,10 +625,10 @@
             dma((count,)),
             dma((tps,)),
             dma((tps,)),
-            dma((2, at.deep)),
-            dma((at.deep,)),
-            dma((at.deep, at.flat)),
-            dma((at.deep, at.flat)),
+            dma((2, at.deep, halves)),
+            dma((at.deep, halves)),
+            dma((at.deep, at.flat, halves)),
+            dma((at.deep, at.flat, halves)),
             dma((at.deep, at.flat, parts)),
             dma((at.deep, at.flat, parts)),
             dma((at.deep, parts)),
@@ -619,12 +642,13 @@
         key_matrix,
         value_matrix,
         channel_decay_input,
-        head_decay_offset,
+        head_decay_offset.T,
         output_gate_input,
         head_norm_gain.reshape(1, -1),
         residual,
         expert_norm_gain.reshape(1, -1),
-        packet,
+        routes.T,
+        chosen_router_scores.T,
         mixer_output_weight,
         *common,
         *routed,

time: 136 us -> 119 us (0.88); the launches traced: 134 us -> 119 us
  Pallas kernels: 128 us -> 118 us
  local copies, waits for them, and re-layouts: 3.42 us -> 0.8 us
  other arithmetic: 1.96 us -> 0 us
    pallas_call x1, Pallas kernels: 128 us -> 118 us  [on_device(): pl.pallas_call(functools.partial(layer_kernel, sizes), out_shape=pltpu.VM...]
    unnamed x2 -> x1, local copies, waits for them, and re-layouts: 3.42 us -> 0.8 us
where the time goes in v4:
time: 119 us
  Pallas kernels  118 us (99%)
    pallas_call x1, Pallas kernels, on_device(): pl.pallas_call(functools.partial(layer_kernel, sizes), out_shape=pltpu.VM...  118 us

profile of v4, /device:TPU:18, one launch (start us, length us, event | category | flops | bytes accessed | tf_op | source)
XLA Modules:
  0.0 119.0 jit_solution(17286637649183754881)
XLA Ops:
  0.0 118.2 %shard_map.172 = bf16[128,2048]{1,0:T(8,128)(2,1)S(1)} custom-call(bf16[512,128]{1,0:T(8,128)(2,1)} %q_ref.1, bf16[512,128]{1,0:T(8,128)(2,1)} %k_ref.1, bf16[512,256]{1,0:T(8,128)(2,1)} %v_ref.1, bf16[512,128]{1,0:T(8,128)(2,1)} %decay_ref.1, f32[2,512]{1,0:T(2,128)} %bitcast.6, bf16[512,256]{1,0:T(8,128)(2,1)} %open_ref.1, f32[1,128]{1,0:T(1,128)} %bitcast.9, ...), custom_call_target="tpu_custom_call" | custom-call | tf_op jit(solution)/shard_map/pallas_call | solution.py:575
  118.2 0.8 copy.20

commit v5 on v4

--- a/solution.py
+++ b/solution.py
@@ -114,7 +114,7 @@
     sizes, q_ref, k_ref, v_ref, decay_ref, offset_ref, open_ref, head_gain_ref, residual_ref,
     gain_ref, routes_ref, scores_ref, far_mix, far_gate, far_up, far_down,
     wide_gate, wide_up, wide_down, out_ref,
-    qd_ref, qx_ref, kg_ref, kt_ref, ends_ref, starts_ref, inner_ref, state_ref, log_ref,
+    qd_ref, qx_ref, kt_ref, ends_ref, starts_ref, inner_ref, state_ref, log_ref,
     states_ref, logs_ref, carried_ref, reach_ref, packet_ref, packets_ref, gated_ref, swapped_ref,
     mixer_ref, x_ref, middle_ref, select_ref, mix_ref,
     column_ref, stage_ref, arrived_ref, made_ref, back_ref, sent_ref, came_ref, base_ref,
@@ -172,10 +172,7 @@
             offset = jnp.where(of_head[h], dropped[:, h : h + 1], offset)
         within = exact_dot(ones, log_decay, dot_nn) + offset
         keys = k_ref[span, :].astype(wide)
-        qd_ref[span, :] = q_ref[span, :].astype(wide) * KEY_CHANNELS ** (-0.5) * jnp.exp(within)
-        grown = keys * jnp.exp(-within)
-        for h in range(heads):
-            kg_ref[h, span, :] = jnp.where(of_head[h], grown, 0.0).astype(half)
+        qd_ref[span, :] = within
         for n in range(0, tile, BLOCK):
             inside = slice(n, n + BLOCK)
             end = within[n + BLOCK - 1 : n + BLOCK, :]
@@ -193,9 +190,6 @@
         added = both[columns[0], :]
         for h in range(1, heads):
             added = jnp.where(of_head[h], both[columns[h], :], added)
-        moved = qd_ref[span, :] * jnp.exp(passed)
-        for h in range(heads):
-            qx_ref[h, span, :] = jnp.where(of_head[h], moved, 0.0).astype(half)
         state = state * jnp.exp(end) + added
         passed = passed + end
     state_ref[...] = state.astype(half)
@@ -228,20 +222,6 @@
     packet_ref[:TOP_K, :] = routes_ref[...].astype(wide)
     packet_ref[TOP_K:, :] = scores_ref[...]
     packets_ref[at.a] = packet_ref[...]
-    for t in range(0, length, tile):
-        span = slice(t, t + tile)
-        ahead = qd_ref[span, :].astype(half)
-        for h in range(heads):
-            scores = jnp.where(causal, dot_nt(ahead, kg_ref[h, span, :]), 0.0)
-            inner_ref[span, columns[h]] = jnp.dot(
-                scores.astype(half), v_ref[span, columns[h]], preferred_element_type=wide
-            )
-    for n in range(1, blocks):
-        span = slice(n * BLOCK, (n + 1) * BLOCK)
-        for h in range(heads):
-            ahead = jnp.where(of_head[h], qd_ref[span, :], 0.0).astype(half)
-            inner_ref[span, columns[h]] += dot_nt(ahead, starts_ref[n])
-
     met()
     for d in range(1, at.deep):
         packet_copy(d).start()
@@ -251,6 +231,29 @@
         def _(d=d):
             for copy in state_copy(d):
                 copy.start()
+
+    for t in range(0, length, tile):
+        span = slice(t, t + tile)
+        within = qd_ref[span, :]
+        grown = k_ref[span, :].astype(wide) * jnp.exp(-within)
+        ahead = q_ref[span, :].astype(wide) * KEY_CHANNELS ** (-0.5) * jnp.exp(within)
+        qd_ref[span, :] = ahead
+        ahead = ahead.astype(half)
+        for h in range(heads):
+            kept = jnp.where(of_head[h], grown, 0.0).astype(half)
+            scores = jnp.where(causal, dot_nt(ahead, kept), 0.0)
+            inner_ref[span, columns[h]] = jnp.dot(
+                scores.astype(half), v_ref[span, columns[h]], preferred_element_type=wide
+            )
+    passed = jnp.zeros((1, lanes), wide)
+    for n in range(blocks):
+        span = slice(n * BLOCK, (n + 1) * BLOCK)
+        for h in range(heads):
+            ahead = jnp.where(of_head[h], qd_ref[span, :], 0.0)
+            qx_ref[h, span, :] = (ahead * jnp.exp(passed)).astype(half)
+            if n > 0:
+                inner_ref[span, columns[h]] += dot_nt(ahead.astype(half), starts_ref[n])
+        passed = passed + ends_ref[n : n + 1, :]
 
     slots = flat * rows
     plane_experts = flat * experts
@@ -305,7 +308,7 @@
             reach_ref[...] += logs_ref[j]
 
     carried = carried_ref[...].astype(half)
-    for d in [*range(1, tps), 0]:
+    for d in [*sorted(range(1, tps), key=lambda d: abs(2 * d - tps)), 0]:
         to = lax.rem(at.tp + d, tps)
         span = pl.ds(pl.multiple_of(to * tokens, tokens), tokens)
         for h in range(heads):
@@ -370,9 +373,19 @@
         return remote(
             stage_ref.at[owner, target, :, sides[j]],
             arrived_ref.at[owner, at.p, :, sides[j]],
-            ps.at[owner, q, j],
-            pr.at[owner, q, j],
+            ps.at[owner, j],
+            pr.at[owner, j],
             at.plane(target),
+        )
+
+    def out_all(owner, j):
+        many = slice(1, flat)
+        return remote(
+            stage_ref.at[owner, many, :, sides[j]],
+            arrived_ref.at[owner, many, :, sides[j]],
+            ps.at[owner, j],
+            pr.at[owner, j],
+            at.plane(at.across(1)),
         )
 
     def back_copy(owner, q, i):
@@ -380,9 +393,19 @@
         return remote(
             made_ref.at[owner, target, :, cuts[i]],
             back_ref.at[owner, at.p, :, cuts[i]],
-            bs.at[owner, q, i],
-            br.at[owner, q, i],
+            bs.at[owner, i],
+            br.at[owner, i],
             at.plane(target),
+        )
+
+    def back_all(owner, i):
+        many = slice(1, flat)
+        return remote(
+            made_ref.at[owner, many, :, cuts[i]],
+            back_ref.at[owner, many, :, cuts[i]],
+            bs.at[owner, i],
+            br.at[owner, i],
+            at.plane(at.across(1)),
         )
 
     def pass_on(owner, source, j):
@@ -401,9 +424,8 @@
             back_copy(owner, q, i).start()
 
     def run_experts(owner):
-        for q in range(1, flat):
-            for j in range(len(sides)):
-                out_copy(owner, q, j).wait_recv()
+        for j in range(len(sides)):
+            out_all(owner, j).wait_recv()
         for e in range(experts):
             mine = slice(e * cap, (e + 1) * cap)
             block = flatten_rows(arrived_ref[owner, :, mine, :])
@@ -425,8 +447,7 @@
             send_back(owner, i)
 
     def mixed(owner, i):
-        for q in range(1, flat):
-            back_copy(owner, q, i).wait_recv()
+        back_all(owner, i).wait_recv()
         block = flatten_rows(back_ref[owner, :, :, cuts[i]])
         return jnp.dot(mix_ref[owner], block, preferred_element_type=jnp.float32)
 
@@ -493,6 +514,34 @@
     for turn in turns[1:]:
         send_all(order[turn])
     send_all(at.a)
+
+    def drain_states(d, carry):
+        @pl.when(at.sp + d < count)
+        def _():
+            for copy in state_copy(d):
+                copy.wait_send()
+
+        return carry
+
+    def drain_out(owner, carry):
+        for j in range(len(sides)):
+            out_all(owner, j).wait_send()
+        return carry
+
+    def drain_relay(owner, carry):
+        right, left = sends(owner)
+        for j in range(len(sides)):
+            pl.when(right)(lambda j=j: relay(x_ref, owner, 0, j).wait_send())
+            pl.when(left)(lambda j=j: relay(x_ref, owner, 1, j).wait_send())
+        return carry
+
+    for d in range(1, at.deep):
+        packet_copy(d).wait_send()
+    for d in range(1, tps):
+        swap_copy(d).wait_send()
+    lax.fori_loop(1, count, drain_states, 0)
+    lax.fori_loop(0, at.deep, drain_relay, 0)
+    lax.fori_loop(0, at.deep, drain_out, 0)
     for turn in turns:
         homeward(turn)
 
@@ -506,31 +555,18 @@
 
     for i, cut in enumerate(cuts):
         out_ref[:, cut] = (base_ref[:, cut] + mixed(at.a, i)).astype(out_ref.dtype)
-    for d in range(1, at.deep):
-        packet_copy(d).wait_send()
-    for d in range(1, count):
-
-        @pl.when(at.sp + d < count)
-        def _(d=d):
-            for copy in state_copy(d):
-                copy.wait_send()
-
-    for d in range(1, tps):
-        swap_copy(d).wait_send()
-    for i in range(at.deep):
-        owner = order[i]
-        right, left = sends(owner)
-        for j in range(len(sides)):
-            pl.when(right)(lambda owner=owner, j=j: relay(x_ref, owner, 0, j).wait_send())
-            pl.when(left)(lambda owner=owner, j=j: relay(x_ref, owner, 1, j).wait_send())
-        for q in range(1, flat):
-            for j in range(len(sides)):
-                out_copy(owner, q, j).wait_send()
-            for j in range(len(cuts)):
-                back_copy(owner, q, j).wait_send()
-        if i > 0:
-            for j in range(len(cuts)):
-                toward(owner, 0, j).wait_send()
+    def drain_back(owner, carry):
+        for j in range(len(cuts)):
+            back_all(owner, j).wait_send()
+        return carry
+
+    def drain_home(owner, carry):
+        for j in range(len(cuts)):
+            pl.when(owner != at.a)(lambda j=j: toward(owner, 0, j).wait_send())
+        return carry
+
+    lax.fori_loop(0, at.deep, drain_back, 0)
+    lax.fori_loop(0, at.deep, drain_home, 0)
 
 
 def on_device(
@@ -580,7 +616,6 @@
         scratch_shapes=[
             pltpu.VMEM((length, lanes), wide),
             pltpu.VMEM((heads, length, lanes), half),
-            pltpu.VMEM((heads, length, lanes), half),
             pltpu.VMEM((length, lanes), half),
             pltpu.VMEM((max(8, blocks), lanes), wide),
             pltpu.VMEM((blocks, VDIM, lanes), half),
@@ -627,10 +662,10 @@
             dma((tps,)),
             dma((2, at.deep, halves)),
             dma((at.deep, halves)),
-            dma((at.deep, at.flat, halves)),
-            dma((at.deep, at.flat, halves)),
-            dma((at.deep, at.flat, parts)),
-            dma((at.deep, at.flat, parts)),
+            dma((at.deep, halves)),
+            dma((at.deep, halves)),
+            dma((at.deep, parts)),
+            dma((at.deep, parts)),
             dma((at.deep, parts)),
             dma((2, at.deep, parts)),
         ],

time: 119 us -> 116 us (0.975)
  Pallas kernels: 118 us -> 115 us
    pallas_call x1, Pallas kernels: 118 us -> 115 us  [on_device(): pl.pallas_call(functools.partial(layer_kernel, sizes), out_shape=pltpu.VM...]
where the time goes in v5:
time: 116 us; the launch traced here: 115 us
  Pallas kernels  115 us (99%)
    pallas_call x1, Pallas kernels, on_device(): pl.pallas_call(functools.partial(layer_kernel, sizes), out_shape=pltpu.VM...  115 us

profile of v5, /device:TPU:18, one launch (start us, length us, event | category | flops | bytes accessed | tf_op | source)
XLA Modules:
  0.0 115.5 jit_solution(16429835983419124987)
XLA Ops:
  0.0 114.7 %shard_map.172 = bf16[128,2048]{1,0:T(8,128)(2,1)S(1)} custom-call(bf16[512,128]{1,0:T(8,128)(2,1)} %q_ref.1, bf16[512,128]{1,0:T(8,128)(2,1)} %k_ref.1, bf16[512,256]{1,0:T(8,128)(2,1)} %v_ref.1, bf16[512,128]{1,0:T(8,128)(2,1)} %decay_ref.1, f32[2,512]{1,0:T(2,128)} %bitcast.6, bf16[512,256]{1,0:T(8,128)(2,1)} %open_ref.1, f32[1,128]{1,0:T(1,128)} %bitcast.9, ...), custom_call_target="tpu_custom_call" | custom-call | tf_op jit(solution)/shard_map/pallas_call | solution.py:611
  114.7 0.8 copy.20

commit v6 on v5

--- a/solution.py
+++ b/solution.py
@@ -111,15 +111,15 @@
 
 
 def layer_kernel(
-    sizes, q_ref, k_ref, v_ref, decay_ref, offset_ref, open_ref, head_gain_ref, residual_ref,
+    sizes, far_q, k_ref, v_ref, decay_ref, offset_ref, far_open, head_gain_ref, far_residual,
     gain_ref, routes_ref, scores_ref, far_mix, far_gate, far_up, far_down,
     wide_gate, wide_up, wide_down, out_ref,
-    qd_ref, qx_ref, kt_ref, ends_ref, starts_ref, inner_ref, state_ref, log_ref,
-    states_ref, logs_ref, carried_ref, reach_ref, packet_ref, packets_ref, gated_ref, swapped_ref,
+    q_ref, open_ref, residual_ref, qd_ref, qx_ref, kt_ref, ends_ref, starts_ref, inner_ref, state_ref,
+    states_ref, carried_ref, reach_ref, packet_ref, packets_ref, gated_ref, swapped_ref,
     mixer_ref, x_ref, middle_ref, select_ref, mix_ref,
     column_ref, stage_ref, arrived_ref, made_ref, back_ref, sent_ref, came_ref, base_ref,
     hidden_ref, shared_ref, gate_ref, up_ref, down_ref, own_gate, own_up, own_down,
-    weight_sem, ks, kr, gs, gr, ls, lr, ws, wr, zs, zr, ps, pr, bs, br, ss, sr,
+    weight_sem, ks, kr, gs, gr, ws, wr, zs, zr, ps, pr, bs, br, ss, sr,
 ):
     at = Place(*sizes).here()
     last = at.deep - 1
@@ -130,6 +130,7 @@
     cuts = tiles_of(width)
     sides = tiles_of(width, 1024)
     pairs = (
+        (far_q, q_ref), (far_open, open_ref), (far_residual, residual_ref),
         (far_mix, mixer_ref), (far_gate, gate_ref), (far_up, up_ref), (far_down, down_ref),
         (wide_gate, own_gate), (wide_up, own_up), (wide_down, own_down),
     )
@@ -192,8 +193,14 @@
             added = jnp.where(of_head[h], both[columns[h], :], added)
         state = state * jnp.exp(end) + added
         passed = passed + end
-    state_ref[...] = state.astype(half)
-    log_ref[...] = jnp.broadcast_to(passed, log_ref.shape)
+    state_ref[:VDIM, :] = state.astype(half)
+    index = lax.broadcasted_iota(jnp.int32, (16, lanes), 0)
+    pieces = jnp.zeros((16, lanes), wide)
+    for i in range(3):
+        piece = passed.astype(half).astype(wide)
+        pieces = jnp.where(index == i, piece, pieces)
+        passed = passed - piece
+    state_ref[VDIM:, :] = pieces.astype(half)
     def packet_copy(d):
         return remote(
             packet_ref,
@@ -208,10 +215,7 @@
 
     def state_copy(d):
         target = peer(jnp.minimum(at.sp + d, count - 1), at.tp)
-        return (
-            remote(state_ref, states_ref.at[at.sp], gs.at[d], gr.at[at.sp], target),
-            remote(log_ref, logs_ref.at[at.sp], ls.at[d], lr.at[at.sp], target),
-        )
+        return remote(state_ref, states_ref.at[at.sp], gs.at[d], gr.at[at.sp], target)
 
     def swap_copy(d):
         to = lax.rem(at.tp + d, tps)
@@ -229,9 +233,9 @@
 
         @pl.when(at.sp + d < count)
         def _(d=d):
-            for copy in state_copy(d):
-                copy.start()
-
+            state_copy(d).start()
+
+    loads[0].wait()
     for t in range(0, length, tile):
         span = slice(t, t + tile)
         within = qd_ref[span, :]
@@ -303,11 +307,12 @@
         def _(j=j):
             source = peer(j, at.tp)
             remote(state_ref, states_ref.at[j], gs.at[0], gr.at[j], source).wait_recv()
-            remote(log_ref, logs_ref.at[j], ls.at[0], lr.at[j], source).wait_recv()
-            carried_ref[...] += jnp.exp(reach_ref[0:1, :]) * states_ref[j].astype(wide)
-            reach_ref[...] += logs_ref[j]
+            carried_ref[...] += jnp.exp(reach_ref[0:1, :]) * states_ref[j, :VDIM, :].astype(wide)
+            log = jnp.sum(states_ref[j, VDIM:, :].astype(wide), axis=0, keepdims=True)
+            reach_ref[0:1, :] += log
 
     carried = carried_ref[...].astype(half)
+    loads[1].wait()
     for d in [*sorted(range(1, tps), key=lambda d: abs(2 * d - tps)), 0]:
         to = lax.rem(at.tp + d, tps)
         span = pl.ds(pl.multiple_of(to * tokens, tokens), tokens)
@@ -324,7 +329,8 @@
             swap_copy(d).start()
     for a in range(early, at.deep):
         lay_out(a)
-    loads[0].wait()
+    for load in loads[2:4]:
+        load.wait()
     span = heads * VDIM
     for d in range(tps):
         source = lax.rem(at.tp - d + tps, tps)
@@ -353,7 +359,7 @@
         return remote(
             source.at[:, sides[j]],
             column_ref.at[owner, :, sides[j]],
-            zs.at[side, owner, j],
+            zs.at[side, owner],
             zr.at[owner, j],
             at.column(at.a + (1 if side == 0 else -1)),
         )
@@ -373,7 +379,7 @@
         return remote(
             stage_ref.at[owner, target, :, sides[j]],
             arrived_ref.at[owner, at.p, :, sides[j]],
-            ps.at[owner, j],
+            ps.at[owner],
             pr.at[owner, j],
             at.plane(target),
         )
@@ -383,7 +389,7 @@
         return remote(
             stage_ref.at[owner, many, :, sides[j]],
             arrived_ref.at[owner, many, :, sides[j]],
-            ps.at[owner, j],
+            ps.at[owner],
             pr.at[owner, j],
             at.plane(at.across(1)),
         )
@@ -393,7 +399,7 @@
         return remote(
             made_ref.at[owner, target, :, cuts[i]],
             back_ref.at[owner, at.p, :, cuts[i]],
-            bs.at[owner, i],
+            bs.at[owner],
             br.at[owner, i],
             at.plane(target),
         )
@@ -403,7 +409,7 @@
         return remote(
             made_ref.at[owner, many, :, cuts[i]],
             back_ref.at[owner, many, :, cuts[i]],
-            bs.at[owner, i],
+            bs.at[owner],
             br.at[owner, i],
             at.plane(at.across(1)),
         )
@@ -455,30 +461,26 @@
         return remote(
             sent_ref.at[owner, :, cuts[i]],
             came_ref.at[side, owner, :, cuts[i]],
-            ss.at[owner, i],
+            ss.at[owner],
             sr.at[side, owner, i],
             at.column(at.a - 1 + 2 * side),
         )
 
-    def step(owner, side, more):
-        for i, cut in enumerate(cuts):
-            part = mixed(owner, i)
-            if more:
-                toward(owner, side, i).wait_recv()
-                part = part + came_ref[side, owner, :, cut].astype(jnp.float32)
-            sent_ref[owner, :, cut] = part.astype(jnp.bfloat16)
-            toward(owner, side, i).start()
-
-    def homeward(turn):
-        for place in range(2):
-            side = jnp.where(2 * at.a < at.deep, 1 - place, place)
-            owner = jnp.where(side == 0, last - turn, turn)
-            goes = jnp.where(side == 0, owner < at.a, owner > at.a)
-            far = jnp.where(side == 0, has_right, has_left)
-            pl.when(goes & far)(lambda owner=owner, side=side: step(owner, side, True))
-            pl.when(goes & jnp.logical_not(far))(
-                lambda owner=owner, side=side: step(owner, side, False)
-            )
+    def step(owner, side, more, i):
+        part = mixed(owner, i)
+        if more:
+            toward(owner, side, i).wait_recv()
+            part = part + came_ref[side, owner, :, cuts[i]].astype(jnp.float32)
+        sent_ref[owner, :, cuts[i]] = part.astype(jnp.bfloat16)
+        toward(owner, side, i).start()
+
+    def homeward(turn, place, i):
+        side = jnp.where(2 * at.a < at.deep, 1 - place, place)
+        owner = jnp.where(side == 0, last - turn, turn)
+        goes = jnp.where(side == 0, owner < at.a, owner > at.a)
+        far = jnp.where(side == 0, has_right, has_left)
+        pl.when(goes & far)(lambda: step(owner, side, True, i))
+        pl.when(goes & jnp.logical_not(far))(lambda: step(owner, side, False, i))
 
     def take(i):
         for j in range(len(sides)):
@@ -491,7 +493,7 @@
         forward(x_ref, at.a, j)
     for j in range(len(sides)):
         pass_on(at.a, x_ref, j)
-    for load in loads[1:4]:
+    for load in loads[4:7]:
         load.wait()
     for cut in tiles_of(gate_ref.shape[1], 256):
         gate = jnp.dot(x_ref[...], gate_ref[:, cut], preferred_element_type=jnp.float32)
@@ -501,38 +503,43 @@
         base_ref[:, cut] = middle_ref[:, cut].astype(jnp.float32) + jnp.dot(
             shared_ref[...], down_ref[:, cut], preferred_element_type=jnp.float32
         )
+    turns = [*range(2, at.deep), 1]
+    early = [turn for turn in turns[:1] if turn < at.deep - 1]
     for i in range(1, at.deep + 1):
         if i < at.deep:
             take(i)
         if i == 1:
-            for load in loads[4:]:
+            for load in loads[7:]:
                 load.wait()
         if i == at.deep:
-            send_all(order[1])
+            for turn in early:
+                send_all(order[turn])
         run_experts(order[i - 1])
-    turns = [1, *range(at.deep - 1, 1, -1)]
-    for turn in turns[1:]:
+    for turn in turns[len(early) :]:
         send_all(order[turn])
     send_all(at.a)
+
+    def sent_all(source, target, sent, came):
+        remote(source, target, sent, came, at.plane(at.across(1))).wait_send()
 
     def drain_states(d, carry):
         @pl.when(at.sp + d < count)
         def _():
-            for copy in state_copy(d):
-                copy.wait_send()
+            state_copy(d).wait_send()
 
         return carry
 
     def drain_out(owner, carry):
-        for j in range(len(sides)):
-            out_all(owner, j).wait_send()
+        sent_all(stage_ref.at[owner, 1:], arrived_ref.at[owner, 1:], ps.at[owner], pr.at[owner, 0])
         return carry
 
     def drain_relay(owner, carry):
-        right, left = sends(owner)
-        for j in range(len(sides)):
-            pl.when(right)(lambda j=j: relay(x_ref, owner, 0, j).wait_send())
-            pl.when(left)(lambda j=j: relay(x_ref, owner, 1, j).wait_send())
+        for side, goes in enumerate(sends(owner)):
+
+            @pl.when(goes)
+            def _(side=side):
+                sent_all(x_ref, column_ref.at[owner], zs.at[side, owner], zr.at[owner, 0])
+
         return carry
 
     for d in range(1, at.deep):
@@ -542,8 +549,14 @@
     lax.fori_loop(1, count, drain_states, 0)
     lax.fori_loop(0, at.deep, drain_relay, 0)
     lax.fori_loop(0, at.deep, drain_out, 0)
-    for turn in turns:
-        homeward(turn)
+    for turn, later in zip(turns, [*turns[1:], None]):
+        if turn == turns[0]:
+            for i in range(len(cuts)):
+                homeward(turn, 0, i)
+        for i in range(len(cuts)):
+            homeward(turn, 1, i)
+            if later is not None:
+                homeward(later, 0, i)
 
     for side, far in ((0, has_right), (1, has_left)):
 
@@ -556,13 +569,14 @@
     for i, cut in enumerate(cuts):
         out_ref[:, cut] = (base_ref[:, cut] + mixed(at.a, i)).astype(out_ref.dtype)
     def drain_back(owner, carry):
-        for j in range(len(cuts)):
-            back_all(owner, j).wait_send()
+        sent_all(made_ref.at[owner, 1:], back_ref.at[owner, 1:], bs.at[owner], br.at[owner, 0])
         return carry
 
     def drain_home(owner, carry):
-        for j in range(len(cuts)):
-            pl.when(owner != at.a)(lambda j=j: toward(owner, 0, j).wait_send())
+        @pl.when(owner != at.a)
+        def _():
+            sent_all(sent_ref.at[owner], came_ref.at[0, owner], ss.at[owner], sr.at[0, owner, 0])
+
         return carry
 
     lax.fori_loop(0, at.deep, drain_back, 0)
@@ -611,19 +625,20 @@
     return pl.pallas_call(
         functools.partial(layer_kernel, sizes),
         out_shape=pltpu.VMEM((tokens, width), half),
-        in_specs=[vmem] * 11 + [far] * 7,
+        in_specs=[far] + [vmem] * 4 + [far, vmem, far] + [vmem] * 3 + [far] * 7,
         out_specs=vmem,
         scratch_shapes=[
+            pltpu.VMEM(queries.shape, half),
+            pltpu.VMEM(output_gate_input.shape, half),
+            pltpu.VMEM(residual.shape, half),
             pltpu.VMEM((length, lanes), wide),
             pltpu.VMEM((heads, length, lanes), half),
             pltpu.VMEM((length, lanes), half),
             pltpu.VMEM((max(8, blocks), lanes), wide),
             pltpu.VMEM((blocks, VDIM, lanes), half),
             pltpu.VMEM((length, heads * VDIM), wide),
-            pltpu.VMEM((VDIM, lanes), half),
-            pltpu.VMEM((8, lanes), wide),
-            pltpu.VMEM((count, VDIM, lanes), half),
-            pltpu.VMEM((count, 8, lanes), wide),
+            pltpu.VMEM((VDIM + 16, lanes), half),
+            pltpu.VMEM((count, VDIM + 16, lanes), half),
             pltpu.VMEM((VDIM, lanes), wide),
             pltpu.VMEM((8, lanes), wide),
             pltpu.VMEM((2 * TOP_K, tokens), wide),
@@ -651,22 +666,20 @@
             pltpu.VMEM(routed[0].shape, half),
             pltpu.VMEM(routed[1].shape, half),
             pltpu.VMEM(routed[2].shape, half),
-            dma((7,)),
+            dma((10,)),
             dma((at.deep,)),
             dma((at.deep,)),
             dma((count,)),
             dma((count,)),
-            dma((count,)),
-            dma((count,)),
             dma((tps,)),
             dma((tps,)),
-            dma((2, at.deep, halves)),
+            dma((2, at.deep)),
             dma((at.deep, halves)),
+            dma((at.deep,)),
             dma((at.deep, halves)),
-            dma((at.deep, halves)),
+            dma((at.deep,)),
             dma((at.deep, parts)),
-            dma((at.deep, parts)),
-            dma((at.deep, parts)),
+            dma((at.deep,)),
             dma((2, at.deep, parts)),
         ],
         compiler_params=pltpu.CompilerParams(

time: 116 us -> 112 us (0.966); the launches traced: 115 us -> 110 us
  Pallas kernels: 115 us -> 110 us
    pallas_call x1, Pallas kernels: 115 us -> 110 us  [on_device(): pl.pallas_call(functools.partial(layer_kernel, sizes), out_shape=pltpu.VM...]
where the time goes in v6:
time: 112 us; the launch traced here: 110 us
  Pallas kernels  110 us (98%)
    pallas_call x1, Pallas kernels, on_device(): pl.pallas_call(functools.partial(layer_kernel, sizes), out_shape=pltpu.VM...  110 us

profile of v6, /device:TPU:18, one launch (start us, length us, event | category | flops | bytes accessed | tf_op | source)
XLA Modules:
  0.0 110.3 jit_solution(977548433659229962)
XLA Ops:
  0.0 109.5 %shard_map.172 = bf16[128,2048]{1,0:T(8,128)(2,1)S(1)} custom-call(bf16[512,128]{1,0:T(8,128)(2,1)} %far_q.1, bf16[512,128]{1,0:T(8,128)(2,1)} %k_ref.1, bf16[512,256]{1,0:T(8,128)(2,1)} %v_ref.1, bf16[512,128]{1,0:T(8,128)(2,1)} %decay_ref.1, f32[2,512]{1,0:T(2,128)} %bitcast.6, bf16[512,256]{1,0:T(8,128)(2,1)} %far_open.1, f32[1,128]{1,0:T(1,128)} %bitcast.9, ...), custom_call_target="tpu_custom_call" | custom-call | tf_op jit(solution)/shard_map/pallas_call | solution.py:625
  109.5 0.8 copy.20

commit v7 on v6

--- a/solution.py
+++ b/solution.py
@@ -278,7 +278,7 @@
         0.0,
     ).astype(half)
     def lay_out(a):
-        pl.when(at.a != a)(lambda a=a: packet_from(a).wait_recv())
+        pl.when(at.a != a)(lambda: packet_from(a).wait_recv())
         scored = packets_ref[a, TOP_K:, :]
         share = routed_scale * scored / jnp.sum(scored, axis=0, keepdims=True)
         chosen = jnp.zeros((plane_experts, tokens), wide)
@@ -296,8 +296,8 @@
         mix_ref[a] = jnp.transpose(jnp.where(taken, weights, 0.0)).astype(half)
 
     early = at.deep // 2
-    for a in range(early):
-        lay_out(a)
+    for i in range(early):
+        lay_out(at.nearest(i))
 
     carried_ref[...] = jnp.zeros_like(carried_ref)
     reach_ref[...] = jnp.zeros_like(reach_ref)
@@ -327,8 +327,8 @@
             ).astype(half)
         if d > 0:
             swap_copy(d).start()
-    for a in range(early, at.deep):
-        lay_out(a)
+    for i in range(early, at.deep):
+        lay_out(at.nearest(i))
     for load in loads[2:4]:
         load.wait()
     span = heads * VDIM

time: 112 us -> 112 us (level)
  no operation moved by 1% of the time
where the time goes in v7:
time: 112 us; the launch traced here: 110 us
  Pallas kernels  110 us (98%)
    pallas_call x1, Pallas kernels, on_device(): pl.pallas_call(functools.partial(layer_kernel, sizes), out_shape=pltpu.VM...  110 us

profile of v7, /device:TPU:18, one launch (start us, length us, event | category | flops | bytes accessed | tf_op | source)
XLA Modules:
  0.0 110.3 jit_solution(14344256385678428038)
XLA Ops:
  0.0 109.5 %shard_map.172 = bf16[128,2048]{1,0:T(8,128)(2,1)S(1)} custom-call(bf16[512,128]{1,0:T(8,128)(2,1)} %far_q.1, bf16[512,128]{1,0:T(8,128)(2,1)} %k_ref.1, bf16[512,256]{1,0:T(8,128)(2,1)} %v_ref.1, bf16[512,128]{1,0:T(8,128)(2,1)} %decay_ref.1, f32[2,512]{1,0:T(2,128)} %bitcast.6, bf16[512,256]{1,0:T(8,128)(2,1)} %far_open.1, f32[1,128]{1,0:T(1,128)} %bitcast.9, ...), custom_call_target="tpu_custom_call" | custom-call | tf_op jit(solution)/shard_map/pallas_call | solution.py:625
  109.5 0.8 copy.20
